TPU v7x, 256 devices: a whole 4x4x8 slice. The times are simulated.
256 devices in a mesh: gr: 2 (over z_hi), fs: 16 (over z_lo, x), tp: 8 (over y, core).
Axes of the slice: x: 4, y: 4, z: 8 (z_hi: 2, z_lo: 4; z = z_hi * 4 + z_lo), core: 2. Of those that a mesh axis runs over, the one named last changes fastest.
Arguments:
- prompt: bfloat16 [16384, 2048], P(('gr', 'fs')), may hold values from -6 to 6
- gain_first: float32 [2048], P(('gr', 'fs')), may hold values from 0.1 to 1.9
- gate_first: float32 [2048, 2816], P(('gr', 'fs'), 'tp'), may hold values from -0.125 to 0.125
- up_first: float32 [2048, 2816], P(('gr', 'fs'), 'tp'), may hold values from -0.125 to 0.125
- down_first: float32 [2816, 2048], P(('gr', 'fs'), 'tp'), may hold values from -0.109375 to 0.109375
- gain_second: float32 [2048], P(('gr', 'fs')), may hold values from 0.1 to 1.9
- gate_second: float32 [2048, 2816], P(('gr', 'fs'), 'tp'), may hold values from -0.125 to 0.125
- up_second: float32 [2048, 2816], P(('gr', 'fs'), 'tp'), may hold values from -0.125 to 0.125
- down_second: float32 [2816, 2048], P(('gr', 'fs'), 'tp'), may hold values from -0.109375 to 0.109375
Outputs:
- serve_gate_first: bfloat16 [2048, 2816], P(None, 'tp')
- serve_up_first: bfloat16 [2048, 2816], P(None, 'tp')
- serve_down_first: bfloat16 [2816, 2048], P('tp')
- serve_gate_second: bfloat16 [2048, 2816], P(None, 'tp')
- serve_up_second: bfloat16 [2048, 2816], P(None, 'tp')
- serve_down_second: bfloat16 [2816, 2048], P('tp')
- mixed: bfloat16 [16384, 2048], P(('gr', 'fs', 'tp'))
All inputs are finite; a program needn't handle non-finite values.
Results may differ from a plain program's by a relative error of at most 0.0085.
Values may be sent and summed in bfloat16 or wider, within the bound.
A program may use at most 128 MiB of HBM per device.

v0:
```python
import jax
import jax.numpy as jnp
from jax import lax
from jax.sharding import PartitionSpec as P


def joined_along(parts, dim):
    parts = jnp.moveaxis(parts, 0, dim)
    dims = parts.shape
    return parts.reshape(*dims[:dim], dims[dim] * dims[dim + 1], *dims[dim + 2 :])


def gather_together(arrays, axis, dims):
    line = jnp.concatenate([a.reshape(-1) for a in arrays])
    lines, at, finished = (lax.all_gather(line, axis), 0, [])
    for a, dim in zip(arrays, dims):
        parts = lines[:, at : at + a.size].reshape(-1, *a.shape)
        finished.append(joined_along(parts, dim))
        at += a.size
    return tuple(finished)


def in_blocks(x, dim, devices):
    dims = x.shape
    parts = x.reshape(*dims[:dim], devices, dims[dim] // devices, *dims[dim + 1 :])
    return jnp.moveaxis(parts, dim, 0)


def sum_at_owner(x, axis, dim):
    devices = lax.axis_size(axis)
    parts = lax.all_to_all(in_blocks(x, dim, devices), axis, 0, 0, tiled=True)
    return jnp.sum(parts.astype(jnp.float32), axis=0)


def normalize(rows):
    rows = rows.astype(jnp.float32)
    scale = lax.rsqrt(jnp.mean(rows * rows, axis=-1, keepdims=True) + 1e-06)
    return (rows * scale).astype(jnp.bfloat16)


def hidden_units(normed, w_gate, w_up):
    gate = jnp.dot(normed, w_gate, preferred_element_type=jnp.float32)
    upper = jnp.dot(normed, w_up, preferred_element_type=jnp.float32)
    return (jax.nn.silu(gate) * upper).astype(jnp.bfloat16)


def rounded_term(hidden, w_down):
    term = jnp.dot(hidden, w_down, preferred_element_type=jnp.float32).astype(jnp.bfloat16)
    return lax.optimization_barrier(term).astype(jnp.float32)


def shards(
    prompt,
    gain_first,
    gate_first,
    up_first,
    down_first,
    gain_second,
    gate_second,
    up_second,
    down_second,
):
    fold_gate_a = (gain_first[:, None] * gate_first).astype(jnp.bfloat16)
    fold_up_a = (gain_first[:, None] * up_first).astype(jnp.bfloat16)
    cast_down_a = down_first.astype(jnp.bfloat16)
    fold_gate_b = (gain_second[:, None] * gate_second).astype(jnp.bfloat16)
    fold_up_b = (gain_second[:, None] * up_second).astype(jnp.bfloat16)
    cast_down_b = down_second.astype(jnp.bfloat16)
    whole = gather_together(
        (fold_gate_a, fold_up_a, cast_down_a, fold_gate_b, fold_up_b, cast_down_b),
        ("gr", "fs"),
        (0, 0, 0, 0, 0, 0),
    )
    gate_a, up_a, tall_a, gate_b, up_b, tall_b = whole
    down_a, down_b = (
        lax.all_to_all(tall_a, "tp", split_axis=0, concat_axis=1, tiled=True),
        lax.all_to_all(tall_b, "tp", split_axis=0, concat_axis=1, tiled=True),
    )
    hidden_a = hidden_units(normalize(prompt), gate_a, up_a)
    branch_a = lax.psum(rounded_term(hidden_a, down_a).astype(jnp.bfloat16), "tp").astype(
        jnp.float32
    )
    stream = prompt.astype(jnp.float32) + 0.5 * branch_a
    hidden_b = hidden_units(normalize(stream), gate_b, up_b)
    owned = hidden_b.shape[0] // lax.axis_size("tp")
    branch_b = sum_at_owner(rounded_term(hidden_b, down_b).astype(jnp.bfloat16), "tp", 0)
    own_stream = lax.dynamic_slice_in_dim(stream, lax.axis_index("tp") * owned, owned, 0)
    mixed = (own_stream + 0.5 * branch_b).astype(jnp.bfloat16)
    return (gate_a, up_a, down_a, gate_b, up_b, down_b, mixed)


def solution(mesh):
    return jax.shard_map(
        shards,
        mesh=mesh,
        in_specs=(
            P(("gr", "fs"), None),
            P(("gr", "fs")),
            P(("gr", "fs"), "tp"),
            P(("gr", "fs"), "tp"),
            P(("gr", "fs"), "tp"),
            P(("gr", "fs")),
            P(("gr", "fs"), "tp"),
            P(("gr", "fs"), "tp"),
            P(("gr", "fs"), "tp"),
        ),
        out_specs=(
            P(None, "tp"),
            P(None, "tp"),
            P("tp", None),
            P(None, "tp"),
            P(None, "tp"),
            P("tp", None),
            P(("gr", "fs", "tp"), None),
        ),
        check_vma=False,
    )
```

profile of v0, /device:TPU:1, one launch (start us, length us, event | category | flops | bytes accessed | tf_op | source)
XLA Modules:
  0.0 290.3 jit_solution(12751440306381874865)
XLA Ops:
  12.5 102.3 %all-gather.3.cloned.1.call-done = bf16[4325376]{0:T(1024)(128)(2,1)} async-done(((bf16[135168]{0:T(1024)(128)(2,1)}), bf16[4325376]{0:T(1024)(128)(2,1)}) %all-gather.3.cloned.1.call-update) | async-done | bytes 8650768 | tf_op jit(solution)/shard_map/all_gather | solution.py:15
  114.9 8.8 %reshape.68 = bf16[32,135168]{1,0:T(8,128)(2,1)} reshape(bf16[4325376]{0:T(1024)(128)(2,1)} %all-gather.3.cloned.1.call-done) | data formatting | bytes 17301504 | tf_op jit(solution)/shard_map/all_gather | solution.py:15
  123.7 6.0 %fusion.23 = (bf16[32,22528]{1,0:T(8,128)(2,1)}, bf16[32,22528]{1,0:T(8,128)(2,1)}, bf16[32,22528]{1,0:T(8,128)(2,1)}, bf16[32,22528]{1,0:T(8,128)(2,1)S(1)}, bf...) fusion(bf16[32,135168]{1,0:T(8,128)(2,1)} %reshape.68), kind=kLoop, calls=%fused_computation.45 | loop fusion | bytes 17301504 | tf_op jit(solution)/shard_map/slice | solution.py:17
  131.3 5.8 %all-to-all-start = ((bf16[8,352,256]{2,1,0:T(8,128)(2,1)}), bf16[8,352,256]{2,1,0:T(8,128)(2,1)S(1)}, u32[]{:S(2)}, u32[]{:S(2)}) async-start(bf16[8,352,256]{2,1,0:T(8,128)(2,1)} %all_to_all.31), calls=%async_computation | async-start | bytes 2883584 | tf_op jit(solution)/shard_map/all_to_all | solution.py:76
  137.6 4.4 %reshape_reshape.14 = bf16[2048,352]{1,0:T(8,128)(2,1)} reshape(bf16[32,22528]{1,0:T(8,128)(2,1)} %get-tuple-element.33) | data formatting | bytes 2883584 | tf_op jit(solution)/shard_map/reshape;reshape | solution.py:10
  142.0 4.4 %reshape_reshape.15 = bf16[2048,352]{1,0:T(8,128)(2,1)} reshape(bf16[32,22528]{1,0:T(8,128)(2,1)} %get-tuple-element.32) | data formatting | bytes 2883584 | tf_op jit(solution)/shard_map/reshape;reshape | solution.py:10
  146.3 2.6 all_to_all.35
  149.0 3.3 %fusion.6 = f32[512,352]{0,1:T(8,128)} fusion(bf16[2048,352]{1,0:T(8,128)(2,1)} %reshape_reshape.14, bf16[512,2048]{1,0:T(8,128)(2,1)S(1)} %copy-done, f32[512]{0:T(512)S(1)} %add_rsqrt_fusion.1), kind=kOutput, calls=%fused_computation.14 | convolution fusion | flops 741343232 | bytes 4261888 | tf_op jit(solution)/shard_map/dot_general | solution.py:42
  152.3 4.0 %all-to-all-done = bf16[8,352,256]{2,1,0:T(8,128)(2,1)S(1)} async-done(((bf16[8,352,256]{2,1,0:T(8,128)(2,1)}), bf16[8,352,256]{2,1,0:T(8,128)(2,1)S(1)}, u32[]{:S(2)}, u32[]{:S(2)}) %all-to-all-start) | async-done | bytes 1441824 | tf_op jit(solution)/shard_map/all_to_all | solution.py:76
  157.4 4.4 %all-to-all-start.1 = ((bf16[8,352,256]{2,1,0:T(8,128)(2,1)}), bf16[8,352,256]{2,1,0:T(8,128)(2,1)S(1)}, u32[]{:S(2)}, u32[]{:S(2)}) async-start(bf16[8,352,256]{2,1,0:T(8,128)(2,1)} %all_to_all.35), calls=%async_computation.1 | async-start | bytes 2883584 | tf_op jit(solution)/shard_map/all_to_all | solution.py:77
  161.8 2.6 copy.32
  164.5 5.7 %convolution_convert_fusion.1 = bf16[512,2048]{1,0:T(8,128)(2,1)} fusion(bf16[352,2048]{1,0:T(8,128)(2,1)} %bitcast.22, bf16[2048,352]{1,0:T(8,128)(2,1)} %reshape_reshape.15, bf16[512,2048]{1,0:T(8,128)(2,1)S(1)} %copy-done, f32[512]{0:T(512)S(1)} %add_rsqrt_fusion.1, f32[512,352]{0,1:T(8,128)} %fusion.6), kind=kOutput, calls=%fused_computation.9 | convolution fusion | flops 1481670656 | bytes 7800832 | tf_op jit(solution)/shard_map/dot_general | solution.py:48
  170.2 4.4 %reshape_reshape.16 = bf16[2048,352]{1,0:T(8,128)(2,1)} reshape(bf16[32,22528]{1,0:T(8,128)(2,1)} %get-tuple-element.30) | data formatting | bytes 2883584 | tf_op jit(solution)/shard_map/reshape;reshape | solution.py:10
  174.6 4.3 %reshape_reshape.17 = bf16[2048,352]{1,0:T(8,128)(2,1)} reshape(bf16[32,22528]{1,0:T(8,128)(2,1)} %get-tuple-element.29) | data formatting | bytes 2883584 | tf_op jit(solution)/shard_map/reshape;reshape | solution.py:10
  178.9 2.1 all-to-all-done.1
  182.3 53.9 %all-reduce.2.cloned.1.call-done = bf16[512,2048]{1,0:T(8,128)(2,1)} async-done(((bf16[512,2048]{1,0:T(8,128)(2,1)}), bf16[512,2048]{1,0:T(8,128)(2,1)}) %all-reduce.2.cloned.1.call-update) | async-done | bytes 2097168 | tf_op jit(solution)/shard_map/psum | solution.py:80
  236.2 4.5 %convert_add_fusion = (f32[512,2048]{1,0:T(8,128)}, f32[512]{0:T(512)S(1)}) fusion(bf16[512,2048]{1,0:T(8,128)(2,1)S(1)} %copy-done, bf16[512,2048]{1,0:T(8,128)(2,1)} %all-reduce.2.cloned.1.call-done), kind=kLoop, calls=%fused_computation | loop fusion | flops 6290944 | bytes 8390656 | tf_op jit(solution)/shard_map/add | solution.py:83
  242.9 6.1 %convolution_convert_fusion = bf16[512,2048]{1,0:T(8,128)(2,1)} fusion(bf16[352,2048]{1,0:T(8,128)(2,1)S(1)} %bitcast.25, bf16[2048,352]{1,0:T(8,128)(2,1)} %reshape_reshape.17, f32[512,352]{0,1:T(8,128)} %fusion.22, f32[512]{0:T(512)S(1)} %add_rsqrt_fusion, bf16[512,2048]{1,0:T(8,128)(2,1)S(1)} %copy-done, bf16[512,2048]{1,0:T(8,128)(2,1)} %all-reduce.2.cloned.1.call-done), kind=kOutput, calls=%fused_computation.8 | convolution fusion | flops 1484816384 | bytes 9897984 | tf_op jit(solution)/shard_map/dot_general | solution.py:48
  249.0 6.1 %all-to-all-start.2 = ((bf16[8,64,2048]{2,1,0:T(8,128)(2,1)}), bf16[8,64,2048]{2,1,0:T(8,128)(2,1)S(1)}, u32[]{:S(2)}, u32[]{:S(2)}) async-start(bf16[8,64,2048]{2,1,0:T(8,128)(2,1)} %bitcast.21), calls=%async_computation.2 | async-start | bytes 4194304 | tf_op jit(solution)/shard_map/all_to_all | solution.py:31
  255.0 2.5 copy.28
  257.6 2.5 copy.29
  260.1 2.5 copy.30
  262.7 2.5 copy.31
  265.2 16.1 %all-to-all-done.2 = bf16[8,64,2048]{2,1,0:T(8,128)(2,1)S(1)} async-done(((bf16[8,64,2048]{2,1,0:T(8,128)(2,1)}), bf16[8,64,2048]{2,1,0:T(8,128)(2,1)S(1)}, u32[]{:S(2)}, u32[]{:S(2)}) %all-to-all-start.2) | async-done | bytes 2097184 | tf_op jit(solution)/shard_map/all_to_all | solution.py:31
  (40 shorter events, 14.0 us)
Async XLA Ops:
  7.2 107.7 %all-gather.3.cloned.1.call-start = ((), (), s32[]{:S(2)}) async-start(), calls=%async_computation.4 | async-start | bytes 8921088 | tf_op jit(solution)/shard_map/all_gather | solution.py:15
  11.8 0.7 copy-start.5
  131.3 5.8 %copy-start = (bf16[512,2048]{1,0:T(8,128)(2,1)S(1)}, bf16[512,2048]{1,0:T(8,128)(2,1)}, u32[]{:S(2)}) copy-start(bf16[512,2048]{1,0:T(8,128)(2,1)} %param.9) | copy-start | bytes 6291460
  131.3 25.0 %all-to-all-start = ((bf16[8,352,256]{2,1,0:T(8,128)(2,1)}), bf16[8,352,256]{2,1,0:T(8,128)(2,1)S(1)}, u32[]{:S(2)}, u32[]{:S(2)}) async-start(bf16[8,352,256]{2,1,0:T(8,128)(2,1)} %all_to_all.31), calls=%async_computation | async-start | bytes 2883584 | tf_op jit(solution)/shard_map/all_to_all | solution.py:76
  156.3 1.1 copy-start.2
  157.4 23.7 %all-to-all-start.1 = ((bf16[8,352,256]{2,1,0:T(8,128)(2,1)}), bf16[8,352,256]{2,1,0:T(8,128)(2,1)S(1)}, u32[]{:S(2)}, u32[]{:S(2)}) async-start(bf16[8,352,256]{2,1,0:T(8,128)(2,1)} %all_to_all.35), calls=%async_computation.1 | async-start | bytes 2883584 | tf_op jit(solution)/shard_map/all_to_all | solution.py:77
  161.8 74.4 %all-reduce.2.cloned.1.call-start = ((), (), s32[]{:S(2)}) async-start(), calls=%async_computation.3 | async-start | bytes 4194304 | tf_op jit(solution)/shard_map/psum | solution.py:80
  236.2 4.5 %copy-start.1 = (bf16[2048,352]{1,0:T(8,128)(2,1)S(1)}, bf16[2048,352]{1,0:T(8,128)(2,1)}, u32[]{:S(2)}) copy-start(bf16[2048,352]{1,0:T(8,128)(2,1)} %reshape_reshape.16) | copy-start | bytes 4325380
  236.2 4.5 %copy-start.3 = (bf16[512,2048]{1,0:T(8,128)(2,1)S(1)}, bf16[512,2048]{1,0:T(8,128)(2,1)}, u32[]{:S(2)}) copy-start(bf16[512,2048]{1,0:T(8,128)(2,1)} %all-reduce.2.cloned.1.call-done) | copy-start | bytes 6291460
  240.8 2.1 copy-start.4
  249.0 32.3 %all-to-all-start.2 = ((bf16[8,64,2048]{2,1,0:T(8,128)(2,1)}), bf16[8,64,2048]{2,1,0:T(8,128)(2,1)S(1)}, u32[]{:S(2)}, u32[]{:S(2)}) async-start(bf16[8,64,2048]{2,1,0:T(8,128)(2,1)} %bitcast.21), calls=%async_computation.2 | async-start | bytes 4194304 | tf_op jit(solution)/shard_map/all_to_all | solution.py:31
Sparse Core Ops, SparseCore 0:
  12.7 102.1 all-gather.2
  170.3 65.8 all-reduce.1
where the time goes:
time: 291 us; the launch traced here: 290 us
  waiting for transfers between devices  179 us (62%)
  local copies, waits for them, and re-layouts  53.1 us (18%)
  matrix products  17.2 us (6%)
  starting transfers between devices  16.4 us (6%)
  between operations  14.1 us (5%)
  other arithmetic  11 us (4%)
    all_gather x1, waiting for transfers between devices, gather_together(): lines, at, finished = (lax.all_gather(line, axis), 0, [])  102 us
    psum x1, waiting for transfers between devices, shards(): lax.psum(rounded_term(hidden_a, down_a).astype(jnp.bfloat16), 'tp')  53.9 us
    another operation x4, local copies, waits for them, and re-layouts, joined_along(): parts.reshape(*dims[:dim], dims[dim] * dims[dim + 1], *dims[dim + 2:])  17.5 us
    all_to_all x1, waiting for transfers between devices, sum_at_owner(): parts = lax.all_to_all(in_blocks(x, dim, devices), axis, 0, 0, tiled=True)  16.1 us
    unnamed x23, local copies, waits for them, and re-layouts  12.1 us
    dot_general x2, matrix products, rounded_term(): jnp.dot(hidden, w_down, preferred_element_type=jnp.float32)  11.8 us
    all_gather x1, local copies, waits for them, and re-layouts, gather_together(): lines, at, finished = (lax.all_gather(line, axis), 0, [])  8.84 us
    all_to_all x1, starting transfers between devices, sum_at_owner(): parts = lax.all_to_all(in_blocks(x, dim, devices), axis, 0, 0, tiled=True)  6.05 us
  transfers between devices with their start and end apart: 5, of which 5 were waited for; matrix products, arithmetic and copies ran while one was open for 14% of the time, Pallas kernels for 0%

commit v1 on v0

v1 whole, which is shorter than its diff:
```python
import functools
import heapq

import jax
import jax.numpy as jnp
from jax import lax
from jax.experimental import pallas as pl
from jax.experimental.pallas import tpu as pltpu
from jax.sharding import PartitionSpec as P

MESH = pl.DeviceIdType.MESH
F32, BF16 = jnp.float32, jnp.bfloat16
NX, NY, NZ = 4, 4, 8
CHUNKS = 4

UNIT = 1.05
WIRE = 1.9
DOWN = 2.1
ROWS = 5.7
PAIR = 0.5


class Copy:
    def __init__(self, name, link, dur, **at):
        self.name, self.link, self.dur, self.at = name, link, dur, at
        self.idx = None


class Plan:
    def __init__(self):
        self.copies, self.tasks = {}, {}

    def copy(self, name, link, dur, late=0.0, **at):
        c = Copy(name, link, dur, **at)
        c.idx, c.late = len(self.copies), late
        self.copies[name] = c
        return c

    def task(self, name, needs, dur, sends=(), rank=0):
        self.tasks[name] = (set(needs), dur, list(sends), rank)

    def order(self):
        users = {}
        left = {}
        for name, (needs, *_) in self.tasks.items():
            left[name] = set(needs)
            for n in needs:
                users.setdefault(n, []).append(name)
        free, ready, coming, seq, now = {}, [], [], 0, 0.0
        for pos, name in enumerate(self.tasks):
            if not left[name]:
                heapq.heappush(ready, (self.tasks[name][3], pos, name))
        place = {name: pos for pos, name in enumerate(self.tasks)}
        done, times = [], {}

        def happened(event, at):
            times[event] = at
            for name in users.get(event, ()):
                left[name].discard(event)
                if not left[name]:
                    heapq.heappush(ready, (self.tasks[name][3], place[name] if self.tasks[name][3] else at, name))

        while ready or coming:
            while coming and (coming[0][0] <= now or not ready):
                at, _, event = heapq.heappop(coming)
                now = max(now, at)
                happened(event, at)
            if not ready:
                continue
            _, _, name = heapq.heappop(ready)
            _, dur, sends, _ = self.tasks[name]
            now += dur
            done.append(name)
            for c in sends:
                c = self.copies[c]
                end = max(now, free.get(c.link, 0.0)) + c.dur
                free[c.link] = end
                wire = 0.9 if c.link == "pair" else WIRE
                seq += 1
                heapq.heappush(coming, (end + wire + c.late, seq, c.name))
            happened(name, now)
        if len(done) != len(self.tasks):
            raise ValueError("plan stuck")
        self.times, self.total = times, now
        return done


def flip(link):
    return link[0] + ("-" if link[1] == "+" else "+")


def build_plan():
    p = Plan()
    whole = {0: [], 1: []}
    down_all = {0: [], 1: []}

    for l in (0, 1):
        after = ["begin"] if l == 0 else ["next"]
        g, u = f"G{l}", f"U{l}"
        have = whole[l]

        def put(buf, link, zrel, xrel, half, tag, have=have):
            dur = UNIT * (0.5 if half is not None else 1.0)
            c = p.copy(f"{buf}:{tag}", link, dur, buf=buf, z=zrel, x=xrel, half=half)
            have.append(c.name)
            return c.name

        first = []
        chain = []
        for s in ("+", "-"):
            sign = -1 if s == "+" else 1
            first.append(put(g, "z" + s, sign, 0, None, f"z{s}1"))
        for s in ("+", "-"):
            sign = -1 if s == "+" else 1
            first.append(put(u, "x" + s, 0, sign, None, f"x{s}"))
        for s in ("+", "-"):
            sign = -1 if s == "+" else 1
            first.append(put(u, "z" + s, sign, 0, None, f"o:z{s}1"))
        for s in ("+", "-"):
            sign = -1 if s == "+" else 1
            first.append(put(g, "x" + s, 0, sign, None, f"own:x{s}"))
        p.task(f"start{l}", after, 0.3, first)

        for s in ("+", "-"):
            sign = -1 if s == "+" else 1
            half = 0 if s == "+" else 1
            p.task(f"{g}fwd:own{s}", [f"{g}:own:x{s}"], 0.03, [put(g, "x" + s, 0, 2, half, f"own:xx{s}")])
            for step in (1, 2, 3, 4):
                src = f"{g}:z{s}{step}"
                zrel = sign * step
                h = half if step == 4 else None
                sends = []
                if step < 4:
                    nh = half if step == 3 else None
                    sends.append(put(g, "z" + s, sign * (step + 1), 0, nh, f"z{s}{step + 1}"))
                for t in ("+", "-"):
                    sends.append(put(g, "x" + t, zrel, -1 if t == "+" else 1, h, f"z{s}{step}:x{t}"))
                p.task(f"{g}fwd:z{s}{step}", [src], 0.03, sends)
                p.task(
                    f"{g}fwd:z{s}{step}x",
                    [f"{g}:z{s}{step}:x{s}"],
                    0.03,
                    [put(g, "x" + s, zrel, 2, h, f"z{s}{step}:xx")],
                )
        for s in ("+", "-"):
            sign = -1 if s == "+" else 1
            half = 0 if s == "+" else 1
            sends = [put(u, "x" + s, 0, 2, half, f"xx{s}")]
            name = "l" if s == "+" else "r"
            for t in ("+", "-"):
                sends.append(put(u, "z" + t, -1 if t == "+" else 1, sign, None, f"{name}:z{t}1"))
            p.task(f"{u}fwd:x{s}", [f"{u}:x{s}"], 0.03, sends)
        sends = [put(u, "z" + t, -1 if t == "+" else 1, 2, None, f"f:z{t}1") for t in ("+", "-")]
        p.task(f"{u}fwd:xx", [f"{u}:xx+", f"{u}:xx-"], 0.03, sends)
        for name, xrel in (("o", 0), ("l", -1), ("r", 1), ("f", 2)):
            for t in ("+", "-"):
                sign = -1 if t == "+" else 1
                last = 4 if (t == "+") == (name in ("o", "r")) else 3
                for step in range(1, last):
                    c = put(u, "z" + t, sign * (step + 1), xrel, None, f"{name}:z{t}{step + 1}")
                    p.task(f"{u}fwd:{name}:z{t}{step}", [f"{u}:{name}:z{t}{step}"], 0.03, [c])

        d = f"D{l}"
        p.copy(f"{d}:own", "y+", 2.0, late=4.0, buf=d, kind="own")
        for k in range(CHUNKS):
            down_all[l].append(p.copy(f"{d}:z+{k}", "z+", DOWN, late=9.0, buf=d, kind="z", chunk=k).name)
            p.copy(f"{d}:z-{k}", "z-", DOWN, buf=d, kind="z", chunk=k)
            for s in ("+", "-"):
                down_all[l].append(
                    p.copy(f"{d}:x{s}{k}", "x" + s, DOWN, buf=d, kind="x", chunk=k, x=-1 if s == "+" else 1).name
                )
            s = "+" if k % 2 == 0 else "-"
            down_all[l].append(p.copy(f"{d}:xx{k}", "x" + s, DOWN, buf=d, kind="x", chunk=k, x=2).name)
            p.task(f"{d}fwd:x{k}", [f"{d}:x{s}{k}"], 0.03, [f"{d}:xx{k}"])
            p.task(f"{d}hop{k}", [f"{d}:z+{k}"], 0.05, [f"{d}:x+{k}", f"{d}:x-{k}"])
        p.task(
            f"{d}src",
            [f"{d}:own", f"U{l}:l:z+2"],
            0.1,
            [f"{d}:z{s}{k}" for k in range(CHUNKS) for s in ("+", "-")],
        )

    p.task("begin", [], 1.0, ["D0:own", "D1:own"])
    p.task("next", ["start0", "D0src", "U0:f:z+2"], 0.02)
    p.task("norm1", ["start0"], 2.0, rank=1)
    p.task("h1", ["norm1"] + whole[0], 3.0, rank=1)
    p.task("asm1", down_all[0], 0.8, rank=1)
    reduce_tasks(p, 0, ["h1", "asm1"], {r: [] for r in range(4)})
    p.copy("N:y+", "y+", ROWS, buf="N", y=-1, half=None, core=0)
    p.copy("N:y-", "y-", ROWS, buf="N", y=1, half=None, core=0)
    p.copy("N:yy+", "y+", ROWS / 2, buf="N", y=2, half=0, core=0)
    p.copy("N:yy-", "y-", ROWS / 2, buf="N", y=2, half=1, core=0)
    p.copy("N:p0", "pair", PAIR, buf="N", y=0, half=None, core=1)
    p.copy("N:p-", "pair", PAIR, buf="N", y=-1, half=None, core=1)
    p.copy("N:p+", "pair", PAIR, buf="N", y=1, half=None, core=1)
    p.copy("N:q0", "pair", PAIR / 2, buf="N", y=2, half=0, core=1)
    p.copy("N:q1", "pair", PAIR / 2, buf="N", y=2, half=1, core=1)
    p.tasks["final0"][2].extend(["N:y+", "N:y-", "N:p0"])
    p.task("Nfwd:+", ["N:y+"], 0.03, ["N:yy+", "N:p-"])
    p.task("Nfwd:-", ["N:y-"], 0.03, ["N:yy-", "N:p+"])
    p.task("Nfwd:h0", ["N:yy+"], 0.03, ["N:q0"])
    p.task("Nfwd:h1", ["N:yy-"], 0.03, ["N:q1"])
    rows = {
        0: ["final0", "N:p0"],
        3: ["N:y+", "N:p-"],
        1: ["N:y-", "N:p+"],
        2: ["N:yy+", "N:yy-", "N:q0", "N:q1"],
    }
    for r in (0, 3, 1, 2):
        p.task(f"h2:{r}", rows[r] + whole[1], 1.3, rank=1)
    p.task("asm2", down_all[1], 0.8, rank=1)
    reduce_tasks(p, 1, ["asm2"], {r: [f"h2:{r}"] for r in range(4)})
    for l in (0, 1):
        p.whole, p.down_all = whole, down_all
    p.sequence = p.order()
    return p


def reduce_tasks(p, l, needs, per):
    for r in (2, 1, 3, 0):
        p.copy(f"R{l}:pair{r}", "pair", PAIR, buf=f"R{l}", kind="pair", rel=r)
        p.task(f"part{l}:{r}", needs + per[r], 0.8, [f"R{l}:pair{r}"], rank=1)
    p.copy(f"R{l}:far+", "y+", ROWS / 2, buf=f"R{l}", kind="far", side=0)
    p.copy(f"R{l}:far-", "y-", ROWS / 2, buf=f"R{l}", kind="far", side=1)
    p.copy(f"R{l}:near+", "y+", ROWS, buf=f"R{l}", kind="near", side=0)
    p.copy(f"R{l}:near-", "y-", ROWS, buf=f"R{l}", kind="near", side=1)
    p.task(f"sum{l}:2", [f"part{l}:2", f"R{l}:pair2"], 0.2, [f"R{l}:far+", f"R{l}:far-"])
    p.task(f"sum{l}:1", [f"part{l}:1", f"R{l}:pair1", f"R{l}:far+"], 0.2, [f"R{l}:near+"])
    p.task(f"sum{l}:3", [f"part{l}:3", f"R{l}:pair3", f"R{l}:far-"], 0.2, [f"R{l}:near-"])
    p.task(f"final{l}", [f"part{l}:0", f"R{l}:pair0", f"R{l}:near+", f"R{l}:near-"], 0.6)


def normalized(rows):
    scale = lax.rsqrt(jnp.mean(rows * rows, axis=-1, keepdims=True) + 1e-06)
    return (rows * scale).astype(BF16)


def gated(normed, w_gate, w_up):
    gate = jnp.dot(normed, w_gate, preferred_element_type=F32)
    upper = jnp.dot(normed, w_up, preferred_element_type=F32)
    return (gate / (1.0 + jnp.exp(-gate)) * upper).astype(BF16)


def kernel(
    plan,
    prompt_hbm,
    gain_a, gate_a, up_a, down_a,
    gain_b, gate_b, up_b, down_b,
    g0, u0, t0, g1, u1, t1, mixed,
    prompt, normed, hidden, part, stream,
    d0, d1, stage, pair0, pair1, far0, far1, near0, near1, sums,
    load_sem, send_sem, recv_sem, own_sem,
):
    gr, fs, tp = lax.axis_index("gr"), lax.axis_index("fs"), lax.axis_index("tp")
    z = gr * 4 + fs // 4
    x = lax.rem(fs, 4)
    y = tp // 2
    core = lax.rem(tp, 2)

    def device(xx, yy, zz, cc):
        return (zz // 4, lax.rem(zz, 4) * 4 + xx, yy * 2 + cc)

    def zat(k):
        return lax.rem(z + (k % NZ), NZ) if k % NZ else z

    def xat(k):
        return lax.rem(x + (k % NX), NX) if k % NX else x

    def yat(k):
        return lax.rem(y + (k % NY), NY) if k % NY else y

    other = 1 - core
    peers = {
        "z+": device(x, y, zat(1), core),
        "z-": device(x, y, zat(-1), core),
        "x+": device(xat(1), y, z, core),
        "x-": device(xat(-1), y, z, core),
        "y+": device(x, yat(1), z, core),
        "y-": device(x, yat(-1), z, core),
        "pair": device(x, y, z, other),
    }
    steps = {"z+": (1, 0, 0), "z-": (-1, 0, 0), "x+": (0, 1, 0), "x-": (0, -1, 0), "y+": (0, 0, 1), "y-": (0, 0, -1), "pair": (0, 0, 0)}
    weights = {"G0": g0, "U0": u0, "G1": g1, "U1": u1}
    downs = {"D0": d0, "D1": d1}
    pairs, fars, nears = (pair0, pair1), (far0, far1), (near0, near1)
    dist = lax.rem(z + NZ - tp, NZ)

    def refs(c, sender):
        dz, dx, dy = steps[c.link] if sender else (0, 0, 0)
        at = c.at
        buf = at["buf"]
        if buf in weights:
            row = (zat(at["z"] + dz) * NX + xat(at["x"] + dx)) * 64
            size = 64
            if at["half"] is not None:
                row, size = row + 32 * at["half"], 32
            ref = weights[buf].at[pl.ds(pl.multiple_of(row, 32), size), :]
            return ref, ref
        if buf in downs:
            n = 8 // CHUNKS
            xx = xat(at.get("x", 0) + dx)
            ref = downs[buf].at[xx, pl.ds(at["chunk"] * n, n)]
            return ref, ref
        if buf == "N":
            cc = core if (at["core"] == 0) == (True) else None
            if at["core"] == 1:
                cc = core if sender else other
            row = (yat(at["y"] + dy) * 2 + cc) * 64
            size = 64
            if at["half"] is not None:
                row, size = row + 32 * at["half"], 32
            ref = normed.at[pl.ds(pl.multiple_of(row, 32), size), :]
            return ref, ref
        l = int(buf[1])
        if at["kind"] == "pair":
            row = (yat(at["rel"]) * 2 + other) * 64
            return part.at[l, pl.ds(pl.multiple_of(row, 64), 64), :], pairs[l].at[at["rel"]]
        if at["kind"] == "far":
            s = at["side"]
            return sums.at[l, 2, pl.ds(32 * s, 32), :], fars[l].at[s]
        s = at["side"]
        return sums.at[l, 1 if s == 0 else 3], nears[l].at[s]

    def describe(c, sender):
        src, dst = refs(c, sender)
        return pltpu.make_async_remote_copy(
            src_ref=src,
            dst_ref=dst,
            send_sem=send_sem.at[c.idx],
            recv_sem=recv_sem.at[c.idx],
            device_id=peers[c.link],
            device_id_type=MESH,
        )

    def own_copy(l):
        return pltpu.make_async_remote_copy(
            src_ref=stage.at[l],
            dst_ref=downs[f"D{l}"].at[x, tp],
            send_sem=send_sem.at[plan.copies[f"D{l}:own"].idx],
            recv_sem=own_sem.at[l, tp],
            device_id=device(x, z // 2, z, lax.rem(z, 2)),
            device_id_type=MESH,
        )

    def down_sends(c, first=None):
        here = dist == 0
        if c.link == "z+":
            later = jnp.logical_and(dist > 0, dist < 4)
        else:
            later = dist > 5
        if first is None:
            return jnp.logical_or(here, later)
        return here if first else later

    def send(name, first=False):
        c = plan.copies[name]
        if c.at["buf"] in downs:
            if c.at["kind"] == "own":
                l = int(c.at["buf"][1])

                @pl.when(tp != z)
                def _():
                    own_copy(l).start()

                return
            if c.at["kind"] == "z":

                @pl.when(down_sends(c, first))
                def _():
                    describe(c, True).start()

                return
        describe(c, True).start()

    def sent(c):
        if c.at["buf"] in downs:
            if c.at["kind"] == "own":

                @pl.when(tp != z)
                def _():
                    own_copy(int(c.at["buf"][1])).wait_send()

                return
            if c.at["kind"] == "z":

                @pl.when(down_sends(c))
                def _():
                    describe(c, True).wait_send()

                return
        describe(c, True).wait_send()

    seen = set()

    def arrived(name):
        if name in seen or name not in plan.copies:
            return
        seen.add(name)
        c = plan.copies[name]
        if c.at["buf"] in downs and c.at["kind"] in ("own", "z"):
            if c.at["kind"] == "own":
                l = int(c.at["buf"][1])
                for t in range(8):

                    @pl.when(jnp.logical_and(dist == 0, tp != t))
                    def _(t=t):
                        pltpu.make_async_remote_copy(
                            src_ref=stage.at[l],
                            dst_ref=downs[c.at["buf"]].at[x, t],
                            send_sem=send_sem.at[c.idx],
                            recv_sem=own_sem.at[l, t],
                            device_id=peers["pair"],
                            device_id_type=MESH,
                        ).wait_recv()

                return
            back = plan.copies[name.replace("z+", "z-")]

            @pl.when(jnp.logical_and(dist > 0, dist < 5))
            def _():
                describe(c, False).wait_recv()

            @pl.when(dist > 4)
            def _():
                describe(back, False).wait_recv()

            return
        describe(c, False).wait_recv()

    eye = lax.broadcasted_iota(jnp.int32, (64, 64), 0) == lax.broadcasted_iota(jnp.int32, (64, 64), 1)

    def fold(gain, w):
        column = jnp.sum(jnp.where(eye, gain[...], 0.0), axis=1, keepdims=True)
        return (column * w[...]).astype(BF16)

    mine = pl.ds(pl.multiple_of((z * NX + x) * 64, 64), 64)

    def rows_of(r):
        return pl.ds(pl.multiple_of(yat(r) * 128, 128), 128)

    def block_of(r, cc):
        return pl.ds(pl.multiple_of((yat(r) * 2 + cc) * 64, 64), 64)

    load = pltpu.make_async_copy(prompt_hbm, prompt, load_sem)

    def begin():
        load.start()
        barrier = pltpu.get_barrier_semaphore()
        greet = [peers[k] for k in ("z+", "z-", "x+", "x-")]
        greet += [(gr, fs, lax.rem(tp + k, 8)) for k in range(1, 8)]
        for who in greet:
            pl.semaphore_signal(barrier, inc=1, device_id=who, device_id_type=MESH)
        g0[mine, :] = fold(gain_a, gate_a)
        u0[mine, :] = fold(gain_a, up_a)
        g1[mine, :] = fold(gain_b, gate_b)
        u1[mine, :] = fold(gain_b, up_b)
        for l, (src, dst) in enumerate(((down_a, d0), (down_b, d1))):
            stage[l] = src[...].astype(BF16)

            @pl.when(tp == z)
            def _(src=src, dst=dst):
                dst[x, tp] = src[...].astype(BF16)

        pl.semaphore_wait(barrier, len(greet))

    def norm1():
        load.wait()

        @pl.loop(0, 8)
        def _(i):
            at = pl.ds(pl.multiple_of(i * 64, 64), 64)
            normed[at, :] = normalized(prompt[at, :].astype(F32))

    def h1():
        @pl.loop(0, 2)
        def _(i):
            at = pl.ds(pl.multiple_of(i * 256, 256), 256)
            hidden[at, :] = gated(normed[at, :], g0[...], u0[...])

    def h2(r):
        at = rows_of(r)
        hidden[at, :] = gated(normed[at, :], g1[...], u1[...])

    def assemble(src, dst):
        for t in range(8):
            rows = jnp.concatenate([src[k, t].astype(F32) for k in range(NX)], axis=0)
            dst[:, 256 * t : 256 * (t + 1)] = rows.astype(BF16)

    def partial(l, r):
        at = rows_of(r)
        w = (t0, t1)[l]
        part[l, at, :] = jnp.dot(hidden[at, :], w[...], preferred_element_type=F32).astype(BF16)

    def chip_sum(l, r):
        return part[l, block_of(r, core), :].astype(F32) + pairs[l][r].astype(F32)

    def add_up(l, r):
        total = chip_sum(l, r)
        if r == 2:
            sums[l, 2] = total.astype(BF16)
            return
        side = 0 if r == 1 else 1
        at, rest = (slice(0, 32), slice(32, 64)) if side == 0 else (slice(32, 64), slice(0, 32))
        sums[l, r, at, :] = (total[at] + fars[l][side].astype(F32)).astype(BF16)
        sums[l, r, rest, :] = total[rest].astype(BF16)

    def final(l):
        total = chip_sum(l, 0) + nears[l][0].astype(F32) + nears[l][1].astype(F32)
        if l == 0:
            at = block_of(0, core)
            rows = prompt[at, :].astype(F32) + 0.5 * total
            stream[...] = rows
            normed[at, :] = normalized(rows)
        else:
            mixed[...] = (stream[...] + 0.5 * total).astype(BF16)

    for name in plan.sequence:
        needs, _, sends, _ = plan.tasks[name]
        for n in plan.copies:
            if n in needs:
                arrived(n)
        with jax.named_scope(name.split(":")[0]):
            if name == "begin":
                begin()
            elif name == "norm1":
                norm1()
            elif name == "h1":
                h1()
            elif name.startswith("h2:"):
                h2(int(name[3]))
            elif name == "asm1":
                assemble(d0, t0)
            elif name == "asm2":
                assemble(d1, t1)
            elif name.startswith("part"):
                partial(int(name[4]), int(name[6]))
            elif name.startswith("sum"):
                add_up(int(name[3]), int(name[5]))
            elif name.startswith("final"):
                final(int(name[5]))
        if name[2:5] == "hop":
            send(f"{name[:2]}:z+{name[5:]}")
            send(f"{name[:2]}:z-{name[5:]}")
        for n in sends:
            send(n, name[2:5] == "src")
    for c in plan.copies.values():
        sent(c)


def shards(prompt, gain_first, gate_first, up_first, down_first, gain_second, gate_second, up_second, down_second):
    plan = build_plan()
    rows, width = prompt.shape
    units = gate_first.shape[1]
    depth, columns = down_first.shape
    count = len(plan.copies)
    vmem = pl.BlockSpec(memory_space=pltpu.VMEM)
    gate_shape = jax.ShapeDtypeStruct((width, units), BF16)
    down_shape = jax.ShapeDtypeStruct((units, width), BF16)
    sem = pltpu.SemaphoreType.DMA
    block = rows // 8
    outs = pl.pallas_call(
        functools.partial(kernel, plan),
        out_shape=(gate_shape, gate_shape, down_shape, gate_shape, gate_shape, down_shape, jax.ShapeDtypeStruct((block, width), BF16)),
        in_specs=[pl.BlockSpec(memory_space=pl.ANY)] + [vmem] * 8,
        out_specs=(vmem,) * 7,
        scratch_shapes=[
            pltpu.VMEM((rows, width), BF16),
            pltpu.VMEM((rows, width), BF16),
            pltpu.VMEM((rows, units), BF16),
            pltpu.VMEM((2, rows, width), BF16),
            pltpu.VMEM((block, width), F32),
            pltpu.VMEM((NX, 8, depth, columns), BF16),
            pltpu.VMEM((NX, 8, depth, columns), BF16),
            pltpu.VMEM((2, depth, columns), BF16),
            pltpu.VMEM((NY, block, width), BF16),
            pltpu.VMEM((NY, block, width), BF16),
            pltpu.VMEM((2, block // 2, width), BF16),
            pltpu.VMEM((2, block // 2, width), BF16),
            pltpu.VMEM((2, block, width), BF16),
            pltpu.VMEM((2, block, width), BF16),
            pltpu.VMEM((2, NY, block, width), BF16),
            sem,
            sem((count,)),
            sem((count,)),
            sem((2, 8)),
        ],
        compiler_params=pltpu.CompilerParams(collective_id=0, has_side_effects=True, vmem_limit_bytes=48 * 1024 * 1024),
        name="handover",
    )(
        prompt,
        gain_first.reshape(1, -1), gate_first, up_first, down_first,
        gain_second.reshape(1, -1), gate_second, up_second, down_second,
    )
    return outs


def solution(mesh):
    rows = P(("gr", "fs"), None)
    block = P(("gr", "fs"), "tp")
    line = P(("gr", "fs"))
    return jax.shard_map(
        shards,
        mesh=mesh,
        in_specs=(rows, line, block, block, block, line, block, block, block),
        out_specs=(
            P(None, "tp"),
            P(None, "tp"),
            P("tp", None),
            P(None, "tp"),
            P(None, "tp"),
            P("tp", None),
            P(("gr", "fs", "tp"), None),
        ),
        check_vma=False,
    )
```

time: 291 us -> 144 us (0.49)
  waiting for transfers between devices: 179 us -> 0 us
  Pallas kernels: 0 us -> 124 us
  local copies, waits for them, and re-layouts: 53.1 us -> 19.1 us
  matrix products: 17.2 us -> 0 us
  starting transfers between devices: 16.4 us -> 0 us
  between operations: 14.1 us -> 0.67 us
  other arithmetic: 11 us -> 0 us
    pallas_call x0 -> x1, Pallas kernels: none -> 124 us  [shards(): pl.pallas_call(functools.partial(kernel, plan), out_shape=(gate_shape, ga...]
    all_gather x1 -> x0, waiting for transfers between devices: 102 us -> none  [gather_together(): lines, at, finished = (lax.all_gather(line, axis), 0, [])]
    psum x1 -> x0, waiting for transfers between devices: 53.9 us -> none  [shards(): lax.psum(rounded_term(hidden_a, down_a).astype(jnp.bfloat16), 'tp')]
    all_to_all x3 -> x0, waiting for transfers between devices: 22.2 us -> none  [the longest x1 16.1 us: sum_at_owner(): parts = lax.all_to_all(in_blocks(x, dim, devices), axis, 0, 0, tiled=True)]
    another operation x4 -> x0, local copies, waits for them, and re-layouts: 17.5 us -> none  [joined_along(): parts.reshape(*dims[:dim], dims[dim] * dims[dim + 1], *dims[dim + 2:])]
    dot_general x4 -> x0, matrix products: 17.2 us -> none  [the longest x2 11.8 us: rounded_term(): jnp.dot(hidden, w_down, preferred_element_type=jnp.float32)]
    all_to_all x3 -> x0, starting transfers between devices: 16.3 us -> none  [the longest x1 6.05 us: sum_at_owner(): parts = lax.all_to_all(in_blocks(x, dim, devices), axis, 0, 0, tiled=True)]
    all_gather x1 -> x0, local copies, waits for them, and re-layouts: 8.84 us -> none  [gather_together(): lines, at, finished = (lax.all_gather(line, axis), 0, [])]
  transfers between devices with their start and end apart: 5 -> 0, of which waited for: 5 -> 0; matrix products, arithmetic and copies ran while one was open for 14% -> 0% of each run, Pallas kernels for 0% -> 0%
where the time goes in v1:
time: 144 us
  Pallas kernels  124 us (86%)
  local copies, waits for them, and re-layouts  19.1 us (13%)
    pallas_call x1, Pallas kernels, shards(): pl.pallas_call(functools.partial(kernel, plan), out_shape=(gate_shape, ga...  124 us
    unnamed x25, local copies, waits for them, and re-layouts  10.7 us
    pallas_call x4, local copies, waits for them, and re-layouts, shards(): pl.pallas_call(functools.partial(kernel, plan), out_shape=(gate_shape, ga...  8.46 us

profile of v1, /device:TPU:1, one launch (start us, length us, event | category | flops | bytes accessed | tf_op | source)
XLA Modules:
  0.0 144.1 jit_solution(15116461584144077103)
XLA Ops:
  0.6 0.0 copy-start.2
  0.6 0.9 copy-done.2
  1.5 0.0 copy-start.3
  1.5 0.9 copy-done.3
  2.4 0.0 copy-start.4
  2.4 0.9 copy-done.4
  3.3 0.0 copy-start.5
  3.3 0.9 copy-done.5
  4.2 0.9 copy-done.6
  5.1 0.9 copy-done.7
  6.0 0.7 copy-done.8
  6.6 0.7 copy-done.9
  7.3 124.3 %handover.1 = (bf16[2048,352]{1,0:T(8,128)(2,1)S(1)}, bf16[2048,352]{1,0:T(8,128)(2,1)}, bf16[352,2048]{1,0:T(8,128)(2,1)S(1)}, bf16[2048,352]{1,0:T(8,128)(2,1)...) custom-call(bf16[512,2048]{1,0:T(8,128)(2,1)} %prompt_hbm.1, ...), custom_call_target="tpu_custom_call" | custom-call | tf_op jit(solution)/shard_map/handover/pallas_call | solution.py:561
  131.6 0.0 copy-start
  131.6 1.1 copy-done
  132.7 1.6 %copy.16 = bf16[2048,352]{0,1:T(8,128)(2,1)} copy(bf16[2048,352]{1,0:T(8,128)(2,1)S(1)} %get-tuple-element.7) | data formatting | bytes 2883584 | tf_op jit(solution)/shard_map/handover/pallas_call | solution.py:561
  134.3 2.7 %copy.17 = bf16[2048,352]{0,1:T(8,128)(2,1)} copy(bf16[2048,352]{1,0:T(8,128)(2,1)} %get-tuple-element.8) | data formatting | bytes 2883584 | tf_op jit(solution)/shard_map/handover/pallas_call | solution.py:561
  136.9 0.0 copy-done.10
  136.9 1.6 %copy.18 = bf16[2048,352]{0,1:T(8,128)(2,1)} copy(bf16[2048,352]{1,0:T(8,128)(2,1)S(1)} %copy-done.10) | data formatting | bytes 2883584 | tf_op jit(solution)/shard_map/handover/pallas_call | solution.py:561
  138.5 2.6 %copy.19 = bf16[2048,352]{0,1:T(8,128)(2,1)} copy(bf16[2048,352]{1,0:T(8,128)(2,1)} %get-tuple-element.11) | data formatting | bytes 2883584 | tf_op jit(solution)/shard_map/handover/pallas_call | solution.py:561
  141.2 0.0 copy-done.1
  141.2 1.1 copy.23
  142.3 1.1 copy.24
  143.4 0.7 copy.25
  (6 shorter events, 0.0 us)
Async XLA Ops:
  0.6 0.9 copy-start.2
  1.5 0.9 copy-start.3
  2.4 0.9 copy-start.4
  3.3 0.9 copy-start.5
  4.2 0.9 copy-start.6
  5.1 0.9 copy-start.7
  6.0 0.7 copy-start.8
  6.6 0.7 copy-start.9
  131.6 1.1 copy-start
  134.3 2.7 %copy-start.10 = (bf16[2048,352]{1,0:T(8,128)(2,1)S(1)}, bf16[2048,352]{1,0:T(8,128)(2,1)}, u32[]{:S(2)}) copy-start(bf16[2048,352]{1,0:T(8,128)(2,1)} %get-tuple-element.10) | copy-start | bytes 4325380
  138.5 2.7 %copy-start.1 = (bf16[352,2048]{1,0:T(8,128)(2,1)S(1)}, bf16[352,2048]{1,0:T(8,128)(2,1)}, u32[]{:S(2)}) copy-start(bf16[352,2048]{1,0:T(8,128)(2,1)} %copy-done) | copy-start | bytes 4325380

commit v2 on v0

v2 whole, which is shorter than its diff:
```python
import functools
import heapq

import jax
import jax.numpy as jnp
from jax import lax
from jax.experimental import pallas as pl
from jax.experimental.pallas import tpu as pltpu
from jax.sharding import PartitionSpec as P

MESH = pl.DeviceIdType.MESH
F32, BF16 = jnp.float32, jnp.bfloat16
NX, NY, NZ = 4, 4, 8
CHUNKS = 4

UNIT, DOWN, ROWS, PAIR, WIRE, NEAR = 1.08, 2.15, 5.7, 0.5, 2.0, 1.0

ZP, ZM, XP, XM, YP, YM, PR = LINKS = range(7)
STEP = {ZP: (1, 0, 0), ZM: (-1, 0, 0), XP: (0, 1, 0), XM: (0, -1, 0), YP: (0, 0, 1), YM: (0, 0, -1), PR: (0, 0, 0)}
G, U, D, N, R = range(5)
BEGIN, START, NORM, HIDE, GLUE, TURN, PART, SUM, LAST, SOURCE, PASS = range(100, 111)
OWN, ALONG, ACROSS, PAIRED, FAR, CLOSE = range(200, 206)


class Copy:
    def __init__(self, idx, link, dur, at):
        self.idx, self.link, self.dur = idx, link, dur
        self.buf = at["buf"]
        self.at = at


class Task:
    def __init__(self, needs, dur, sends, rank, only):
        self.needs, self.dur, self.sends, self.rank, self.only = list(needs), dur, list(sends), rank, only

    def falls_to(self, d):
        return self.only is None or min(d, NZ - d) == self.only


class Plan:
    def __init__(self):
        self.copies, self.tasks = {}, {}

    def copy(self, key, link, dur, **at):
        self.copies[key] = Copy(len(self.copies), link, dur, at)
        return key

    def task(self, key, needs, dur, sends=(), rank=0, only=None):
        self.tasks[key] = Task(needs, dur, sends, rank, only)

    def issues(self, key, d):
        for c in self.tasks[key].sends:
            copy = self.copies[c]
            if copy.buf == D and copy.at["kind"] == ALONG and not goes_on(copy.link, d):
                continue
            yield c, copy

    def absent(self, need, d):
        if need in self.tasks:
            return not self.tasks[need].falls_to(d)
        copy = self.copies.get(need)
        if copy is None or copy.buf != D:
            return False
        if copy.at["kind"] == OWN:
            return d != 0
        return copy.at["kind"] == ALONG and (d == 0 or (copy.link == ZP) != (d < 5))

    def simulate(self, fixed=None):
        kinds = [(d, c) for d in range(NZ) for c in range(2)]
        left = {k: {t: {n for n in v.needs if not self.absent(n, k[0])} for t, v in self.tasks.items() if v.falls_to(k[0])} for k in kinds}
        users = {}
        for t, v in self.tasks.items():
            for n in v.needs:
                users.setdefault(n, []).append(t)
        place = {t: i for i, t in enumerate(fixed or self.tasks)}
        ready = {k: [] for k in kinds}
        free = {}
        busy = {k: 0.0 for k in kinds}
        done = {k: {} for k in kinds}
        turn = {k: 0 for k in kinds}
        events, seq = [], 0

        def settle(k, need, at):
            done[k].setdefault(need, at)
            for t in users.get(need, ()):
                if need in left[k].get(t, ()):
                    left[k][t].discard(need)
                    if not left[k][t]:
                        heapq.heappush(ready[k], (self.tasks[t].rank, place[t] if self.tasks[t].rank else at, place[t], t))

        for k in kinds:
            for t in left[k]:
                if not left[k][t]:
                    heapq.heappush(ready[k], (self.tasks[t].rank, 0.0, place[t], t))
            heapq.heappush(events, (0.0, seq, k, None))
            seq += 1
        starts = {k: {} for k in kinds}
        while events:
            now, _, k, what = heapq.heappop(events)
            if what is not None:
                settle(k, what, now)
            if now < busy[k]:
                continue
            if fixed is None:
                if not ready[k]:
                    continue
                t = heapq.heappop(ready[k])[3]
            else:
                while turn[k] < len(fixed) and fixed[turn[k]] not in left[k]:
                    turn[k] += 1
                if turn[k] == len(fixed) or left[k][fixed[turn[k]]]:
                    continue
                t = fixed[turn[k]]
                turn[k] += 1
            starts[k][t] = now
            end = now + self.tasks[t].dur
            busy[k] = end
            d, c = k
            for name, copy in self.issues(t, d):
                at = max(end, free.get((k, copy.link), 0.0)) + copy.dur
                free[k, copy.link] = at
                dz, _, dy = STEP[copy.link]
                to = ((d + dz - 2 * dy) % NZ, c)
                if copy.buf == D and copy.at["kind"] == OWN:
                    to = (0, c)
                if copy.link == PR:
                    to = ((d + (-1 if c == 0 else 1)) % NZ, 1 - c)
                seq += 1
                heapq.heappush(events, (at + (NEAR if copy.link == PR else WIRE), seq, to, name))
            seq += 1
            heapq.heappush(events, (end, seq, k, t))
        return starts, max(busy.values())

    def line_up(self, starts, mix):
        at = {}
        for t in self.tasks:
            here = [v[t] for v in starts.values() if t in v]
            at[t] = mix * max(here) + (1 - mix) * sum(here) / len(here)
        place = {t: i for i, t in enumerate(self.tasks)}
        changed = True
        while changed:
            changed = False
            for t, before in self.before.items():
                for n in before:
                    if at[n] >= at[t]:
                        at[t] = at[n] + 1e-6
                        changed = True
        return sorted(self.tasks, key=lambda t: (at[t], place[t]))

    def find_before(self):
        starters, self.before = {}, {}
        for t, v in self.tasks.items():
            for c in v.sends:
                starters.setdefault(c, []).append(t)
        for t, v in self.tasks.items():
            before = [n for n in v.needs if n in self.tasks]
            for n in v.needs:
                for y in starters.get(n, ()):
                    hop = self.copies[n].buf == D and self.copies[n].at["kind"] == ALONG
                    m = self.tasks[y].only
                    if m is None or v.only is None or m == v.only - hop:
                        before.append(y)
            self.before[t] = before

    def order(self):
        self.find_before()
        starts, self.ideal = self.simulate()
        best = None
        for mix in (0.0, 0.2, 0.4, 0.6, 0.8, 1.0):
            line = self.line_up(starts, mix)
            total = self.simulate(line)[1]
            if best is None or total < best[0]:
                best = total, line
        self.total = best[0]
        return best[1]


def goes_on(link, d):
    return d < 4 if link == ZP else d == 0 or d > 5


RELEASE = [1, 2, 3, 0, 5, 2, 2, 7]


def mark(l, place):
    if place == 0:
        return (START, l)
    if place < 5:
        return (PASS, G, l, ALONG, 0, place)
    if place < 7:
        return (PASS, U, l, ALONG, 0, 0, place - 4)
    if place < 9:
        return (PASS, U, l, ALONG, 3, 0, place - 6)
    return (PASS, D, l, ACROSS, place - 9, 4)


def build_plan():
    p = Plan()
    whole, downs = ([], []), ([], [])
    signs = ((0, -1), (1, 1))
    zs, xs = (ZP, ZM), (XP, XM)

    p.task((BEGIN,), [], 3.0, [p.copy((D, l, OWN), YP, 2.0, buf=D, layer=l, kind=OWN) for l in (0, 1)])
    for l in (0, 1):

        def put(buf, link, zrel, xrel, half, *tag):
            key = (buf, l, *tag)
            whole[l].append(p.copy(key, link, UNIT * (1.0 if half is None else 0.5), buf=buf, layer=l, z=zrel, x=xrel, half=half))
            return key

        first = [put(G, zs[s], sign, 0, None, ALONG, s, 1) for s, sign in signs]
        first += [put(U, xs[s], 0, sign, None, ACROSS, s) for s, sign in signs]
        first += [put(U, zs[s], sign, 0, None, ALONG, 0, s, 1) for s, sign in signs]
        first += [put(G, xs[s], 0, sign, None, OWN, s) for s, sign in signs]
        p.task((START, l), [(BEGIN,)] if l == 0 else [mark(0, RELEASE[3 + CHUNKS])], 0.2, first)

        for s, sign in signs:
            p.task((PASS, G, l, OWN, s), [(G, l, OWN, s)], 0.03, [put(G, xs[s], 0, 2, s, OWN, s, 2)])
            for step in (1, 2, 3, 4):
                zrel, half = sign * step, s if step == 4 else None
                sends = []
                if step < 4:
                    sends.append(put(G, zs[s], sign * (step + 1), 0, s if step == 3 else None, ALONG, s, step + 1))
                for t, to in signs:
                    sends.append(put(G, xs[t], zrel, to, half, ACROSS, s, step, t))
                p.task((PASS, G, l, ALONG, s, step), [(G, l, ALONG, s, step)], 0.03, sends)
                p.task((PASS, G, l, ACROSS, s, step), [(G, l, ACROSS, s, step, s)], 0.03, [put(G, xs[s], zrel, 2, half, ACROSS, s, step, 2)])
        for s, sign in signs:
            p.task((PASS, U, l, ACROSS, s), [(U, l, ACROSS, s)], 0.03, [put(U, xs[s], 0, 2, s, ACROSS, s, 2)])
            sends = [put(U, zs[t], to, sign, None, ALONG, 1 + s, t, 1) for t, to in signs]
            p.task((PASS, U, l, ALONG, 1 + s), [(U, l, ACROSS, s), mark(l, RELEASE[s])], 0.03, sends)
        sends = [put(U, zs[t], to, 2, None, ALONG, 3, t, 1) for t, to in signs]
        p.task((PASS, U, l, ALONG, 3), [(U, l, ACROSS, 0, 2), (U, l, ACROSS, 1, 2), mark(l, RELEASE[2])], 0.03, sends)
        for column, xrel in enumerate((0, -1, 1, 2)):
            for t, sign in signs:
                for step in range(1, 4 if (t == 0) == (column in (0, 2)) else 3):
                    c = put(U, zs[t], sign * (step + 1), xrel, None, ALONG, column, t, step + 1)
                    p.task((PASS, U, l, ALONG, column, t, step), [(U, l, ALONG, column, t, step)], 0.03, [c])

        along = {}
        for k in range(CHUNKS):
            for s, sign in signs:
                along[k, s] = p.copy((D, l, ALONG, k, s), zs[s], DOWN, buf=D, layer=l, kind=ALONG, chunk=k)
            sends = [along[k, 0], along[k, 1]]
            sends += [p.copy((D, l, ACROSS, k, s), xs[s], DOWN, buf=D, layer=l, kind=ACROSS, chunk=k, x=sign) for s, sign in signs]
            s = k % 2
            c = p.copy((D, l, ACROSS, k, 2), xs[s], DOWN, buf=D, layer=l, kind=ACROSS, chunk=k, x=2)
            for m in range(NZ // 2 + 1):
                needs = [(SOURCE, l), mark(l, RELEASE[3 + k])] if m == 0 else [along[k, 0], along[k, 1]]
                p.task((PASS, D, l, ALONG, k, m), needs, 0.05, sends, only=m)
                p.task((PASS, D, l, ACROSS, k, m), [(D, l, ACROSS, k, s)], 0.03, [c], only=m)
                downs[l].append((PASS, D, l, ALONG, k, m))
            downs[l].extend([sends[2], sends[3], c])
        p.task((SOURCE, l), [(D, l, OWN)], 0.1, [], only=0)

    p.task((NORM,), [(START, 0)], 2.0, rank=1)
    p.task((HIDE, 0), [(NORM,)] + whole[0], 3.0, rank=1)
    p.task((GLUE, 0), downs[0], 0.8, rank=1)
    add_reduce(p, 0, [(HIDE, 0), (GLUE, 0)], {r: [] for r in range(4)})
    for s, sign in signs:
        c = p.copy((N, CLOSE, s), (YP, YM)[s], ROWS, buf=N, y=sign, half=None, core=0)
        p.tasks[LAST, 0].sends.append(c)
        far = p.copy((N, FAR, s), (YP, YM)[s], ROWS / 2, buf=N, y=2, half=s, core=0)
        near = p.copy((N, PAIRED, s), PR, PAIR, buf=N, y=sign, half=None, core=1)
        p.task((PASS, N, CLOSE, s), [c], 0.03, [far, near])
        p.task((PASS, N, FAR, s), [far], 0.03, [p.copy((N, PAIRED, FAR, s), PR, PAIR / 2, buf=N, y=2, half=s, core=1)])
    p.tasks[LAST, 0].sends.append(p.copy((N, PAIRED), PR, PAIR, buf=N, y=0, half=None, core=1))
    rows = {
        0: [(LAST, 0), (N, PAIRED)],
        3: [(N, CLOSE, 0), (N, PAIRED, 0)],
        1: [(N, CLOSE, 1), (N, PAIRED, 1)],
        2: [(N, FAR, 0), (N, FAR, 1), (N, PAIRED, FAR, 0), (N, PAIRED, FAR, 1)],
    }
    for r in (0, 3, 1, 2):
        p.task((HIDE, 1, r), rows[r] + whole[1], 1.3, rank=1)
    p.task((GLUE, 1), downs[1], 0.8, rank=1)
    add_reduce(p, 1, [(GLUE, 1)], {r: [(HIDE, 1, r)] for r in range(4)})
    for l in (0, 1):
        for buf in (G, U):
            for part in (0, 1):
                p.task((TURN, buf, l, part), whole[l] + [(HIDE, 0)], 0.5, rank=2)
    p.sequence = p.order()
    return p


def add_reduce(p, l, needs, per):
    for r in (2, 1, 3, 0):
        c = p.copy((R, l, PAIRED, r), PR, PAIR, buf=R, layer=l, kind=PAIRED, rel=r)
        p.task((PART, l, r), needs + per[r], 0.8, [c], rank=1)
    far = [p.copy((R, l, FAR, s), (YP, YM)[s], ROWS / 2, buf=R, layer=l, kind=FAR, side=s) for s in (0, 1)]
    near = [p.copy((R, l, CLOSE, s), (YP, YM)[s], ROWS, buf=R, layer=l, kind=CLOSE, side=s) for s in (0, 1)]
    p.task((SUM, l, 2), [(PART, l, 2), (R, l, PAIRED, 2)], 0.2, far)
    for s, r in enumerate((1, 3)):
        p.task((SUM, l, r), [(PART, l, r), (R, l, PAIRED, r), far[s]], 0.2, [near[s]])
    p.task((LAST, l), [(PART, l, 0), (R, l, PAIRED, 0)] + near, 0.6)


def normalized(rows):
    scale = lax.rsqrt(jnp.mean(rows * rows, axis=-1, keepdims=True) + 1e-06)
    return (rows * scale).astype(BF16)


def gated(normed, w_gate, w_up):
    gate = jnp.dot(normed, w_gate, preferred_element_type=F32)
    upper = jnp.dot(normed, w_up, preferred_element_type=F32)
    return (gate / (1.0 + jnp.exp(-gate)) * upper).astype(BF16)


def kernel(
    plan,
    prompt_hbm,
    gain_a, gate_a, up_a, down_a,
    gain_b, gate_b, up_b, down_b,
    gt0, ut0, t0, gt1, ut1, t1, mixed,
    prompt, normed, hidden, part, stream,
    g0, u0, g1, u1, d0, d1, stage,
    pair0, pair1, far0, far1, near0, near1, sums,
    gains, gates, depths,
    load_sem, send_sem, recv_sem, own_sem,
):
    gr, fs, tp = lax.axis_index("gr"), lax.axis_index("fs"), lax.axis_index("tp")
    z = gr * 4 + fs // 4
    x = lax.rem(fs, 4)
    y = tp // 2
    core = lax.rem(tp, 2)

    def device(xx, yy, zz, cc):
        return (zz // 4, lax.rem(zz, 4) * 4 + xx, yy * 2 + cc)

    def zat(k):
        return lax.rem(z + (k % NZ), NZ) if k % NZ else z

    def xat(k):
        return lax.rem(x + (k % NX), NX) if k % NX else x

    def yat(k):
        return lax.rem(y + (k % NY), NY) if k % NY else y

    other = 1 - core
    peers = {
        ZP: device(x, y, zat(1), core),
        ZM: device(x, y, zat(-1), core),
        XP: device(xat(1), y, z, core),
        XM: device(xat(-1), y, z, core),
        YP: device(x, yat(1), z, core),
        YM: device(x, yat(-1), z, core),
        PR: device(x, y, z, other),
    }
    weights = {(G, 0): g0, (U, 0): u0, (G, 1): g1, (U, 1): u1}
    turned = {(G, 0): gt0, (U, 0): ut0, (G, 1): gt1, (U, 1): ut1}
    downs, talls = (d0, d1), (t0, t1)
    pairs, fars, nears = (pair0, pair1), (far0, far1), (near0, near1)
    dist = lax.rem(z + NZ - tp, NZ)

    def rows_at(ref, row, half):
        if half is None:
            return ref.at[pl.ds(pl.multiple_of(row, 64), 64), :]
        return ref.at[pl.ds(pl.multiple_of(row + 32 * half, 32), 32), :]

    def refs(c, sender):
        dz, dx, dy = STEP[c.link] if sender else (0, 0, 0)
        at = c.at
        if c.buf in (G, U):
            row = (zat(at["z"] + dz) * NX + xat(at["x"] + dx)) * 64
            ref = rows_at(weights[c.buf, at["layer"]], row, at["half"])
            return ref, ref
        if c.buf == D:
            n = 8 // CHUNKS
            ref = downs[at["layer"]].at[xat(at.get("x", 0) + dx), pl.ds(at["chunk"] * n, n)]
            return ref, ref
        if c.buf == N:
            cc = other if at["core"] and not sender else core
            ref = rows_at(normed, (yat(at["y"] + dy) * 2 + cc) * 64, at["half"])
            return ref, ref
        l = at["layer"]
        if at["kind"] == PAIRED:
            return rows_at(part.at[l], (yat(at["rel"]) * 2 + other) * 64, None), pairs[l].at[at["rel"]]
        side = at["side"]
        if at["kind"] == FAR:
            return sums.at[l, 2, pl.ds(32 * side, 32), :], fars[l].at[side]
        return sums.at[l, 1 + 2 * side], nears[l].at[side]

    def describe(c, sender):
        src, dst = refs(c, sender)
        return pltpu.make_async_remote_copy(
            src_ref=src,
            dst_ref=dst,
            send_sem=send_sem.at[c.idx],
            recv_sem=recv_sem.at[c.idx],
            device_id=peers[c.link],
            device_id_type=MESH,
        )

    def own_copy(c, t):
        l = c.at["layer"]
        return pltpu.make_async_remote_copy(
            src_ref=stage.at[l],
            dst_ref=downs[l].at[x, t],
            send_sem=send_sem.at[c.idx],
            recv_sem=own_sem.at[l, t],
            device_id=device(x, z // 2, z, lax.rem(z, 2)),
            device_id_type=MESH,
        )

    def passes(c):
        if c.buf != D or c.at["kind"] == ACROSS:
            return None
        if c.at["kind"] == OWN:
            return dist != 0
        return dist < 4 if c.link == ZP else jnp.logical_or(dist == 0, dist > 5)

    def if_so(here, act):
        if here is None:
            act()
        else:
            pl.when(here)(act)

    def is_own(c):
        return c.buf == D and c.at["kind"] == OWN

    def send(c, here):
        copy = own_copy(c, tp) if is_own(c) else describe(c, True)
        if_so(here, copy.start)

    def sent(c):
        copy = own_copy(c, tp) if is_own(c) else describe(c, True)
        if_so(passes(c), copy.wait_send)

    seen = set()

    def arrived(key, only):
        c = plan.copies[key]
        if c.buf == D and c.at["kind"] == ALONG:
            if_so(dist == (only if c.link == ZP else NZ - only), describe(c, False).wait_recv)
            return
        if (key, only) in seen or (only is None and (key, 4) in seen):
            return
        seen.add((key, only))
        if is_own(c):
            for t in range(8):
                if_so(jnp.logical_and(dist == 0, tp != t), own_copy(c, t).wait_recv)
            return
        here = None if only is None else hops == only
        if_so(here, describe(c, False).wait_recv)

    hops = jnp.minimum(dist, NZ - dist)
    eye = lax.broadcasted_iota(jnp.int32, (64, 64), 0) == lax.broadcasted_iota(jnp.int32, (64, 64), 1)

    def fold(gain, w):
        column = jnp.sum(jnp.where(eye, gain[...], 0.0), axis=1, keepdims=True)
        return (column * w[...]).astype(BF16)

    mine = pl.ds(pl.multiple_of((z * NX + x) * 64, 64), 64)

    def rows_of(r):
        return pl.ds(pl.multiple_of(yat(r) * 128, 128), 128)

    def block_of(r, cc):
        return pl.ds(pl.multiple_of((yat(r) * 2 + cc) * 64, 64), 64)

    loads = [
        pltpu.make_async_copy(src, dst, load_sem.at[i])
        for i, (src, dst) in enumerate(
            (
                (gain_a, gains.at[0]), (gate_a, gates.at[0]), (up_a, gates.at[1]), (down_a, depths.at[0]),
                (gain_b, gains.at[1]), (gate_b, gates.at[2]), (up_b, gates.at[3]), (down_b, depths.at[1]),
                (prompt_hbm, prompt),
            )
        )
    ]

    def begin():
        for load in loads:
            load.start()
        barrier = pltpu.get_barrier_semaphore()
        greet = [peers[k] for k in (ZP, ZM, XP, XM)]
        greet += [(gr, fs, lax.rem(tp + k, 8)) for k in range(1, 8)]
        for who in greet:
            pl.semaphore_signal(barrier, inc=1, device_id=who, device_id_type=MESH)
        for load in loads[:8]:
            load.wait()
        for i, ref in enumerate((g0, u0, g1, u1)):
            ref[mine, :] = fold(gains.at[i // 2], gates.at[i])
        for l in (0, 1):
            stage[l] = depths[l].astype(BF16)

            @pl.when(dist == 0)
            def _(l=l):
                downs[l][x, tp] = depths[l].astype(BF16)

        pl.semaphore_wait(barrier, len(greet))

    def norm():
        loads[8].wait()

        @pl.loop(0, 8)
        def _(i):
            at = pl.ds(pl.multiple_of(i * 64, 64), 64)
            normed[at, :] = normalized(prompt[at, :].astype(F32))

    def hide(l, r=None):
        if l == 0:

            @pl.loop(0, 2)
            def _(i):
                at = pl.ds(pl.multiple_of(i * 256, 256), 256)
                hidden[at, :] = gated(normed[at, :], g0[...], u0[...])

        else:
            at = rows_of(r)
            hidden[at, :] = gated(normed[at, :], g1[...], u1[...])

    def turn(buf, l, piece):
        src, dst = weights[buf, l], turned[buf, l]

        @pl.loop(0, 4)
        def _(i):
            at = pl.ds(pl.multiple_of((piece * 4 + i) * 256, 256), 256)
            dst[:, at] = src[at, :].astype(F32).T.astype(BF16)

    def glue(l):
        for t in range(8):
            rows = jnp.concatenate([downs[l][k, t].astype(F32) for k in range(NX)], axis=0)
            talls[l][:, 256 * t : 256 * (t + 1)] = rows.astype(BF16)

    def partial(l, r):
        at = rows_of(r)
        part[l, at, :] = jnp.dot(hidden[at, :], talls[l][...], preferred_element_type=F32).astype(BF16)

    def chip_sum(l, r):
        return part[l, block_of(r, core), :].astype(F32) + pairs[l][r].astype(F32)

    def add_up(l, r):
        total = chip_sum(l, r)
        if r == 2:
            sums[l, 2] = total.astype(BF16)
            return
        side = 0 if r == 1 else 1
        at, rest = (slice(0, 32), slice(32, 64)) if side == 0 else (slice(32, 64), slice(0, 32))
        sums[l, r, at, :] = (total[at] + fars[l][side].astype(F32)).astype(BF16)
        sums[l, r, rest, :] = total[rest].astype(BF16)

    def last(l):
        total = chip_sum(l, 0) + nears[l][0].astype(F32) + nears[l][1].astype(F32)
        if l == 0:
            at = block_of(0, core)
            rows = prompt[at, :].astype(F32) + 0.5 * total
            stream[...] = rows
            normed[at, :] = normalized(rows)
        else:
            mixed[...] = (stream[...] + 0.5 * total).astype(BF16)

    work = {BEGIN: begin, NORM: norm, HIDE: hide, TURN: turn, GLUE: glue, PART: partial, SUM: add_up, LAST: last}
    for key in plan.sequence:
        task = plan.tasks[key]
        for n in task.needs:
            if n in plan.copies and not (task.only == 4 and plan.copies[n].link == ZM and plan.copies[n].at.get("kind") == ALONG):
                arrived(n, task.only)
        if key[0] in work:
            work[key[0]](*key[1:])
        for n in task.sends:
            c = plan.copies[n]
            here = passes(c)
            if task.only is not None:
                here = hops == task.only if here is None else jnp.logical_and(here, hops == task.only)
            send(c, here)
    for c in plan.copies.values():
        sent(c)


def hand_out(*refs):
    sources, targets, sem = refs[:7], refs[7:14], refs[14]
    copies = [pltpu.make_async_copy(a, b, sem.at[i]) for i, (a, b) in enumerate(zip(sources, targets))]
    for copy in copies:
        copy.start()
    for copy in copies:
        copy.wait()


def shards(prompt, gain_first, gate_first, up_first, down_first, gain_second, gate_second, up_second, down_second):
    plan = build_plan()
    rows, width = prompt.shape
    units = gate_first.shape[1]
    depth, columns = down_first.shape
    count = len(plan.copies)
    sem, vmem = pltpu.SemaphoreType.DMA, pltpu.VMEM
    block = rows // 8
    tall = jax.ShapeDtypeStruct((units, width), BF16)
    shapes = (tall,) * 6 + (jax.ShapeDtypeStruct((block, width), BF16),)
    outs = pl.pallas_call(
        functools.partial(kernel, plan),
        out_shape=shapes,
        in_specs=[pl.BlockSpec(memory_space=pltpu.HBM)] * 9,
        out_specs=(pl.BlockSpec(memory_space=vmem),) * 7,
        scratch_shapes=[
            vmem((rows, width), BF16),
            vmem((rows, width), BF16),
            vmem((rows, units), BF16),
            vmem((2, rows, width), BF16),
            vmem((block, width), F32),
            *[vmem((width, units), BF16)] * 4,
            *[vmem((NX, 8, depth, columns), BF16)] * 2,
            vmem((2, depth, columns), BF16),
            *[vmem((NY, block, width), BF16)] * 2,
            *[vmem((2, block // 2, width), BF16)] * 2,
            *[vmem((2, block, width), BF16)] * 2,
            vmem((2, NY, block, width), BF16),
            vmem((2, 1, gain_first.shape[0]), F32),
            vmem((4, *gate_first.shape), F32),
            vmem((2, depth, columns), F32),
            sem((9,)),
            sem((count,)),
            sem((count,)),
            sem((2, 8)),
        ],
        compiler_params=pltpu.CompilerParams(collective_id=0, has_side_effects=True, vmem_limit_bytes=LIMIT),
        name="handover",
    )(
        *[
            pltpu.with_memory_space_constraint(a, pltpu.HBM)
            for a in (
                prompt,
                gain_first.reshape(1, -1), gate_first, up_first, down_first,
                gain_second.reshape(1, -1), gate_second, up_second, down_second,
            )
        ],
    )
    outs = pl.pallas_call(
        hand_out,
        out_shape=shapes,
        in_specs=[pl.BlockSpec(memory_space=vmem)] * 7,
        out_specs=(pl.BlockSpec(memory_space=pl.ANY),) * 7,
        scratch_shapes=[sem((7,))],
        compiler_params=pltpu.CompilerParams(vmem_limit_bytes=16 * 1024 * 1024),
        name="hand_out",
    )(*outs)
    return (outs[0].T, outs[1].T, outs[2], outs[3].T, outs[4].T, outs[5], outs[6])


LIMIT = 44 * 1024 * 1024


def solution(mesh):
    rows = P(("gr", "fs"), None)
    block = P(("gr", "fs"), "tp")
    line = P(("gr", "fs"))
    return jax.shard_map(
        shards,
        mesh=mesh,
        in_specs=(rows, line, block, block, block, line, block, block, block),
        out_specs=(
            P(None, "tp"),
            P(None, "tp"),
            P("tp", None),
            P(None, "tp"),
            P(None, "tp"),
            P("tp", None),
            P(("gr", "fs", "tp"), None),
        ),
        check_vma=False,
    )
```

time: 291 us -> 110 us (0.38)
  waiting for transfers between devices: 179 us -> 0 us
  Pallas kernels: 0 us -> 109 us
  local copies, waits for them, and re-layouts: 53.1 us -> 0 us
  matrix products: 17.2 us -> 0 us
  starting transfers between devices: 16.4 us -> 0 us
  between operations: 14.1 us -> 0.64 us
  other arithmetic: 11 us -> 0 us
    pallas_call x0 -> x2, Pallas kernels: none -> 109 us  [the longest x1 105 us: shards(): pl.pallas_call(functools.partial(kernel, plan), out_shape=shapes, in_spec...]
    all_gather x1 -> x0, waiting for transfers between devices: 102 us -> none  [gather_together(): lines, at, finished = (lax.all_gather(line, axis), 0, [])]
    psum x1 -> x0, waiting for transfers between devices: 53.9 us -> none  [shards(): lax.psum(rounded_term(hidden_a, down_a).astype(jnp.bfloat16), 'tp')]
    all_to_all x3 -> x0, waiting for transfers between devices: 22.2 us -> none  [the longest x1 16.1 us: sum_at_owner(): parts = lax.all_to_all(in_blocks(x, dim, devices), axis, 0, 0, tiled=True)]
    another operation x4 -> x0, local copies, waits for them, and re-layouts: 17.5 us -> none  [joined_along(): parts.reshape(*dims[:dim], dims[dim] * dims[dim + 1], *dims[dim + 2:])]
    dot_general x4 -> x0, matrix products: 17.2 us -> none  [the longest x2 11.8 us: rounded_term(): jnp.dot(hidden, w_down, preferred_element_type=jnp.float32)]
    all_to_all x3 -> x0, starting transfers between devices: 16.3 us -> none  [the longest x1 6.05 us: sum_at_owner(): parts = lax.all_to_all(in_blocks(x, dim, devices), axis, 0, 0, tiled=True)]
    unnamed x23 -> x0, local copies, waits for them, and re-layouts: 12.1 us -> none
  transfers between devices with their start and end apart: 5 -> 0, of which waited for: 5 -> 0; matrix products, arithmetic and copies ran while one was open for 14% -> 0% of each run, Pallas kernels for 0% -> 0%
where the time goes in v2:
time: 110 us; the launch traced here: 109 us
  Pallas kernels  109 us (99%)
    pallas_call x1, Pallas kernels, shards(): pl.pallas_call(functools.partial(kernel, plan), out_shape=shapes, in_spec...  105 us
    pallas_call x1, Pallas kernels, shards(): pl.pallas_call(hand_out, out_shape=shapes, in_specs=[pl.BlockSpec(memory_...  3.49 us

profile of v2, /device:TPU:1, one launch (start us, length us, event | category | flops | bytes accessed | tf_op | source)
XLA Modules:
  0.0 109.3 jit_solution(15204261561276932765)
XLA Ops:
  0.6 105.2 %handover.1 = (bf16[352,2048]{1,0:T(8,128)(2,1)S(1)}, bf16[352,2048]{1,0:T(8,128)(2,1)S(1)}, bf16[352,2048]{1,0:T(8,128)(2,1)S(1)}, bf16[352,2048]{1,0:T(8,128)(...) custom-call(bf16[512,2048]{1,0:T(8,128)(2,1)} %prompt_hbm.1, ...), custom_call_target="tpu_custom_call" | custom-call | tf_op jit(solution)/shard_map/handover/pallas_call | solution.py:590
  105.8 3.5 %hand_out.1 = (bf16[352,2048]{1,0:T(8,128)(2,1)}, bf16[352,2048]{1,0:T(8,128)(2,1)}, bf16[352,2048]{1,0:T(8,128)(2,1)}, bf16[352,2048]{1,0:T(8,128)(2,1)}, bf16[...) custom-call(bf16[352,2048]{1,0:T(8,128)(2,1)S(1)} %get-tuple-element.21.refs_0_, ...), custom_call_target="tpu_custom_call" | custom-call | tf_op jit(solution)/shard_map/hand_out/pallas_call | solution.py:628

commit v3 on v2

v3 whole, which is shorter than its diff:
```python
import functools
import heapq

import jax
import jax.numpy as jnp
from jax import lax
from jax.experimental import pallas as pl
from jax.experimental.pallas import tpu as pltpu
from jax.sharding import PartitionSpec as P

MESH = pl.DeviceIdType.MESH
F32, BF16 = jnp.float32, jnp.bfloat16
NX, NY, NZ = 4, 4, 8
CHUNKS = 4
WAVES = 2
WAVE = 64 // WAVES
GROUPS = ((2,), (1, 3), (0,))

UNIT, SQUARE, DOWN, ROWS, PAIR, WIRE, NEAR = 1.08, 1.0, 2.15, 5.7, 0.5, 2.0, 1.0

ZP, ZM, XP, XM, YP, YM, PR = LINKS = range(7)
STEP = {ZP: (1, 0, 0), ZM: (-1, 0, 0), XP: (0, 1, 0), XM: (0, -1, 0), YP: (0, 0, 1), YM: (0, 0, -1), PR: (0, 0, 0)}
G, U, D, N, R, E = range(6)
BEGIN, START, NORM, HIDE, GLUE, TURN, PART, SUM, LAST, SOURCE, PASS = range(100, 111)
OWN, ALONG, ACROSS, PAIRED, FAR, CLOSE, GIVE = range(200, 207)


class Copy:
    def __init__(self, idx, link, dur, at):
        self.idx, self.link, self.dur = idx, link, dur
        self.buf = at["buf"]
        self.at = at
        self.rank = 0


class Task:
    def __init__(self, needs, dur, sends, rank, only):
        self.needs, self.dur, self.sends, self.rank, self.only = list(needs), dur, list(sends), rank, only

    def falls_to(self, d):
        return self.only is None or min(d, NZ - d) == self.only


class Plan:
    def __init__(self):
        self.copies, self.tasks = {}, {}

    def copy(self, key, link, dur, **at):
        self.copies[key] = Copy(len(self.copies), link, dur, at)
        return key

    def task(self, key, needs, dur, sends=(), rank=0, only=None):
        self.tasks[key] = Task(needs, dur, sends, rank, only)

    def starts_here(self, c, d):
        if c.buf != D or c.at["kind"] == ACROSS:
            return True
        if c.at["kind"] == OWN:
            return d != 0
        return d < 4 if c.link == ZP else d == 0 or d > 5

    def absent(self, need, d):
        if need in self.tasks:
            return not self.tasks[need].falls_to(d)
        copy = self.copies.get(need)
        if copy is None or copy.buf != D:
            return False
        if copy.at["kind"] == OWN:
            return d != 0
        return copy.at["kind"] == ALONG and (d == 0 or (copy.link == ZP) != (d < 5))

    def simulate(self, fixed=None):
        kinds = [(d, c) for d in range(NZ) for c in range(2)]
        left = {k: {t: {n for n in v.needs if not self.absent(n, k[0])} for t, v in self.tasks.items() if v.falls_to(k[0])} for k in kinds}
        users = {}
        for t, v in self.tasks.items():
            for n in v.needs:
                users.setdefault(n, []).append(t)
        place = {t: i for i, t in enumerate(self.tasks)}
        ready, pending, turn = {k: [] for k in kinds}, {}, {k: 0 for k in kinds}
        free, busy = {}, {k: 0.0 for k in kinds}
        starts = {k: {} for k in kinds}
        events, self.count = [], 0

        def at_time(at, k, link, what):
            self.count += 1
            heapq.heappush(events, (at, self.count, k, link, what))

        def enable(k, t, at):
            rank = self.tasks[t].rank
            heapq.heappush(ready[k], (rank, place[t] if rank else at, place[t], t))

        def start(k, key, only, now):
            copy = self.copies[key]
            d, c = k
            starts[k][key, only] = now
            end = free[k, copy.link] = max(now, free.get((k, copy.link), 0.0)) + copy.dur
            dz, _, dy = STEP[copy.link]
            to = ((d + dz - 2 * dy) % NZ, c)
            if copy.buf == D and copy.at["kind"] == OWN:
                to = (0, c)
            if copy.link == PR:
                to = ((d + (-1 if c == 0 else 1)) % NZ, 1 - c)
            at_time(end + (NEAR if copy.link == PR else WIRE), to, None, key)

        for k in kinds:
            for t in left[k]:
                if not left[k][t]:
                    enable(k, t, 0.0)
            at_time(0.0, k, None, None)
        while events:
            now, _, k, link, what = heapq.heappop(events)
            if link is not None:
                queue = pending[k, link]
                if queue and now >= free.get((k, link), 0.0) - AHEAD - 1e-9:
                    _, _, key, only = heapq.heappop(queue)
                    start(k, key, only, now)
                if queue:
                    at_time(max(now, free[k, link] - AHEAD), k, link, None)
                continue
            for t in users.get(what, ()) if what is not None else ():
                if what in left[k].get(t, ()):
                    left[k][t].discard(what)
                    if not left[k][t]:
                        enable(k, t, now)
            if what in self.tasks and fixed is None:
                task = self.tasks[what]
                for key in task.sends:
                    copy = self.copies[key]
                    if self.starts_here(copy, k[0]):
                        self.count += 1
                        heapq.heappush(pending.setdefault((k, copy.link), []), (copy.rank, self.count, key, task.only))
                        at_time(max(now, free.get((k, copy.link), 0.0) - AHEAD), k, copy.link, None)
            if now < busy[k]:
                continue
            if fixed is None:
                if not ready[k]:
                    continue
                t = heapq.heappop(ready[k])[3]
            else:
                t = None
                while turn[k] < len(fixed):
                    key, only = fixed[turn[k]]
                    if key in self.tasks:
                        if key in left[k]:
                            if not left[k][key]:
                                t = key
                                turn[k] += 1
                            break
                    elif (only is None or min(k[0], NZ - k[0]) == only) and self.starts_here(self.copies[key], k[0]):
                        start(k, key, only, now)
                    turn[k] += 1
                if t is None:
                    continue
            starts[k][t, None] = now
            busy[k] = now + self.tasks[t].dur
            at_time(busy[k], k, None, t)
        if fixed is not None and any(turn[k] < len(fixed) for k in kinds):
            return starts, 1e9
        return starts, max(busy.values())

    def find_before(self):
        starters, self.before = {}, {}
        for t, v in self.tasks.items():
            for c in v.sends:
                starters.setdefault(c, []).append((c, v.only))
                self.before[c, v.only] = [(t, None)]
        for t, v in self.tasks.items():
            before = [(n, None) for n in v.needs if n in self.tasks]
            for n in v.needs:
                for c, m in starters.get(n, ()):
                    hop = self.copies[n].buf == D and self.copies[n].at["kind"] == ALONG
                    if m is None or v.only is None or m == v.only - hop:
                        before.append((c, m))
            self.before[t, None] = before

    def line_up(self, starts, mix):
        at = {}
        for e in self.before:
            here = [v[e] for v in starts.values() if e in v]
            at[e] = mix * max(here) + (1 - mix) * sum(here) / len(here) if here else 0.0
        place = {e: i for i, e in enumerate(self.before)}
        changed = True
        while changed:
            changed = False
            for e, before in self.before.items():
                for n in before:
                    if at[n] >= at[e]:
                        at[e] = at[n] + 1e-6
                        changed = True
        return sorted(self.before, key=lambda e: (at[e], place[e]))

    def order(self):
        self.find_before()
        starts, self.ideal = self.simulate()
        best = None
        for mix in (0.0, 0.2, 0.4, 0.6, 0.8, 1.0):
            line = self.line_up(starts, mix)
            total = self.simulate(line)[1]
            if best is None or total < best[0]:
                best = total, line
        self.total = best[0]
        return best[1]


GATE = (PASS, G, 1, ALONG, 0, 2)
AHEAD = 2.0
RANKS = [3, 0, -2, 8, 1, 10, 2, 0, 5, 10, 1, 36, 60, -24]


def rank_copies(p):
    for key, c in p.copies.items():
        if c.buf not in (G, U, D, E):
            continue
        l = c.at["layer"]
        if c.link in (YP, YM):
            r = 0
        elif c.link in (ZP, ZM):
            if c.buf == D:
                r = RANKS[0]
            elif c.buf in (G, E):
                r = RANKS[1] + RANKS[2] * key[-1]
            else:
                r = RANKS[3] + RANKS[4] * key[-1]
        elif c.buf == U:
            r = RANKS[5] if len(key) == 4 else RANKS[6]
        elif c.buf in (G, E):
            far = c.at["x"] == 2
            r = RANKS[9] if far else RANKS[7] if key[2] == OWN else RANKS[8]
        else:
            r = RANKS[11] if c.at["x"] == 2 else RANKS[10]
        c.rank = r + RANKS[12] * l + RANKS[13] * (c.buf == E)


def build_plan():
    p = Plan()
    whole, downs, blocks = ([], []), ([], []), {}
    signs = ((0, -1), (1, 1))
    zs, xs = (ZP, ZM), (XP, XM)

    p.task((BEGIN,), [], 3.0, [p.copy((D, 1, OWN), YP, 2.0, buf=D, layer=1, kind=OWN)])
    for l in (0, 1):

        def put(buf, link, zrel, xrel, half, *tag):
            key = (buf, l, *tag)
            unit = SQUARE if buf == E else UNIT
            p.copy(key, link, unit * (1.0 if half is None else 0.5), buf=buf, layer=l, z=zrel, x=xrel, half=half)
            (blocks.setdefault(zrel % NZ, []) if buf == E else whole[l]).append(key)
            return key

        z_first = (G, E) if l == 0 else (G,)
        first = []
        for s, sign in signs:
            first += [put(b, zs[s], sign, 0, None, ALONG, s, 1) for b in z_first]
            first += [put(U, xs[s], 0, sign, None, ACROSS, s)]
            first += [put(U, zs[s], sign, 0, None, ALONG, 0, s, 1)]
            first += [put(b, xs[s], 0, sign, None, OWN, s) for b in z_first]
        p.task((START, l), [(BEGIN,)] if l == 0 else [(START, 0)], 0.2, first)

        for b in z_first:
            for s, sign in signs:
                p.task((PASS, b, l, OWN, s), [(b, l, OWN, s)], 0.03, [put(b, xs[s], 0, 2, s, OWN, s, 2)])
                for step in (1, 2, 3, 4):
                    zrel, half = sign * step, s if step == 4 else None
                    sends = []
                    if step < 4:
                        sends.append(put(b, zs[s], sign * (step + 1), 0, s if step == 3 else None, ALONG, s, step + 1))
                    for t, to in signs:
                        sends.append(put(b, xs[t], zrel, to, half, ACROSS, s, step, t))
                    p.task((PASS, b, l, ALONG, s, step), [(b, l, ALONG, s, step)], 0.03, sends)
                    far = put(b, xs[s], zrel, 2, half, ACROSS, s, step, 2)
                    p.task((PASS, b, l, ACROSS, s, step), [(b, l, ACROSS, s, step, s)], 0.03, [far])
        for s, sign in signs:
            p.task((PASS, U, l, ACROSS, s), [(U, l, ACROSS, s)], 0.03, [put(U, xs[s], 0, 2, s, ACROSS, s, 2)])
            sends = [put(U, zs[t], to, sign, None, ALONG, 1 + s, t, 1) for t, to in signs]
            p.task((PASS, U, l, ALONG, 1 + s), [(U, l, ACROSS, s)], 0.03, sends)
        sends = [put(U, zs[t], to, 2, None, ALONG, 3, t, 1) for t, to in signs]
        p.task((PASS, U, l, ALONG, 3), [(U, l, ACROSS, 0, 2), (U, l, ACROSS, 1, 2)], 0.03, sends)
        for column, xrel in enumerate((0, -1, 1, 2)):
            for t, sign in signs:
                for step in range(1, 4 if (t == 0) == (column in (0, 2)) else 3):
                    c = put(U, zs[t], sign * (step + 1), xrel, None, ALONG, column, t, step + 1)
                    p.task((PASS, U, l, ALONG, column, t, step), [(U, l, ALONG, column, t, step)], 0.03, [c])

    for k in range(NZ):
        c = p.copy((E, 0, GIVE, k), (YP, YM)[k % 2], 3.9, buf=E, layer=0, k=k)
        p.task((PASS, E, 0, GIVE, k), blocks[k], 0.05, [c])
        downs[0].extend([c, (PASS, E, 0, GIVE, k)])
    l, along = 1, {}
    for k in range(CHUNKS):
        for s, sign in signs:
            along[k, s] = p.copy((D, l, ALONG, k, s), zs[s], DOWN, buf=D, layer=l, kind=ALONG, chunk=k)
        sends = [along[k, 0], along[k, 1]]
        sends += [p.copy((D, l, ACROSS, k, s), xs[s], DOWN, buf=D, layer=l, kind=ACROSS, chunk=k, x=sign) for s, sign in signs]
        s = k % 2
        c = p.copy((D, l, ACROSS, k, 2), xs[s], DOWN, buf=D, layer=l, kind=ACROSS, chunk=k, x=2)
        for m in range(NZ // 2 + 1):
            needs = [(SOURCE, l)] if m == 0 else [along[k, 0], along[k, 1]]
            p.task((PASS, D, l, ALONG, k, m), needs, 0.05, sends, only=m)
            p.task((PASS, D, l, ACROSS, k, m), [(D, l, ACROSS, k, s)], 0.03, [c], only=m)
            downs[l].append((PASS, D, l, ALONG, k, m))
        downs[l].extend([sends[2], sends[3], c])
    p.task((SOURCE, l), [(D, l, OWN), GATE], 0.1, [], only=0)

    p.task((NORM,), [(START, 0)], 2.0, rank=1)
    p.task((HIDE, 0), [(NORM,)] + whole[0], 3.0, rank=1)
    p.task((GLUE, 0), downs[0], 0.8, rank=1)
    add_reduce(p, 0, [(HIDE, 0), (GLUE, 0)])
    for w in range(WAVES):
        for s, sign in signs:
            c = p.copy((N, w, CLOSE, s), (YP, YM)[s], ROWS / WAVES, buf=N, wave=w, y=sign, half=None, core=0)
            p.tasks[LAST, 0, w].sends.append(c)
            far = p.copy((N, w, FAR, s), (YP, YM)[s], ROWS / WAVES / 2, buf=N, wave=w, y=2, half=s, core=0)
            near = p.copy((N, w, PAIRED, s), PR, PAIR / WAVES, buf=N, wave=w, y=sign, half=None, core=1)
            p.task((PASS, N, w, CLOSE, s), [c], 0.03, [far, near])
            c = p.copy((N, w, PAIRED, FAR, s), PR, PAIR / WAVES / 2, buf=N, wave=w, y=2, half=s, core=1)
            p.task((PASS, N, w, FAR, s), [far], 0.03, [c])
        p.tasks[LAST, 0, w].sends.append(p.copy((N, w, PAIRED), PR, PAIR / WAVES, buf=N, wave=w, y=0, half=None, core=1))
        rows = {
            (0,): [(LAST, 0, w), (N, w, PAIRED)],
            (1, 3): [(N, w, CLOSE, 0), (N, w, PAIRED, 0), (N, w, CLOSE, 1), (N, w, PAIRED, 1)],
            (2,): [(N, w, FAR, 0), (N, w, FAR, 1), (N, w, PAIRED, FAR, 0), (N, w, PAIRED, FAR, 1)],
        }
        for rs in GROUPS[::-1]:
            p.task((HIDE, 1, w, rs), rows[rs] + whole[1], 1.2, rank=1)
    p.task((GLUE, 1), downs[1], 0.8, rank=1)
    add_reduce(p, 1, [(GLUE, 1)])
    for l in (0, 1):
        for buf in (G, U):
            for part in (0, 1):
                p.task((TURN, buf, l, part), whole[l] + [(HIDE, 0)], 0.5, rank=2)
    rank_copies(p)
    p.sequence = p.order()
    return p


def add_reduce(p, l, needs):
    for w in range(WAVES):
        for rs in GROUPS:
            c = [p.copy((R, l, w, PAIRED, r), PR, PAIR / WAVES, buf=R, layer=l, wave=w, kind=PAIRED, rel=r) for r in rs]
            p.task((PART, l, w, rs), needs + ([(HIDE, 1, w, rs)] if l else []), 0.7, c, rank=1)
        far, near = [
            [p.copy((R, l, w, kind, s), (YP, YM)[s], ROWS / WAVES / part, buf=R, layer=l, wave=w, kind=kind, side=s) for s in (0, 1)]
            for kind, part in ((FAR, 2), (CLOSE, 1))
        ]
        p.task((SUM, l, w, 2), [(PART, l, w, (2,)), (R, l, w, PAIRED, 2)], 0.15, far)
        for s, r in enumerate((1, 3)):
            p.task((SUM, l, w, r), [(PART, l, w, (1, 3)), (R, l, w, PAIRED, r), far[s]], 0.15, [near[s]])
        p.task((LAST, l, w), [(PART, l, w, (0,)), (R, l, w, PAIRED, 0)] + near, 0.4)


def normalized(rows):
    scale = lax.rsqrt(jnp.mean(rows * rows, axis=-1, keepdims=True) + 1e-06)
    return (rows * scale).astype(BF16)


def gated(normed, w_gate, w_up):
    gate = jnp.dot(normed, w_gate, preferred_element_type=F32)
    upper = jnp.dot(normed, w_up, preferred_element_type=F32)
    return (gate / (1.0 + jnp.exp(-gate)) * upper).astype(BF16)


def kernel(
    plan,
    prompt_hbm,
    gain_a, gate_a, up_a, down_a,
    gain_b, gate_b, up_b, down_b,
    gt0, ut0, t0, gt1, ut1, t1, mixed,
    prompt, normed, hidden, part, stream,
    g0, u0, g1, u1, squares, given, d1, stage,
    pair0, pair1, far0, far1, near0, near1, sums,
    gains, gates, depths,
    load_sem, send_sem, recv_sem, own_sem,
):
    gr, fs, tp = lax.axis_index("gr"), lax.axis_index("fs"), lax.axis_index("tp")
    z = gr * 4 + fs // 4
    x = lax.rem(fs, 4)
    y = tp // 2
    core = lax.rem(tp, 2)

    def device(xx, yy, zz, cc):
        return (zz // 4, lax.rem(zz, 4) * 4 + xx, yy * 2 + cc)

    def zat(k):
        return lax.rem(z + (k % NZ), NZ) if k % NZ else z

    def xat(k):
        return lax.rem(x + (k % NX), NX) if k % NX else x

    def yat(k):
        return lax.rem(y + (k % NY), NY) if k % NY else y

    other = 1 - core
    peers = {
        ZP: device(x, y, zat(1), core),
        ZM: device(x, y, zat(-1), core),
        XP: device(xat(1), y, z, core),
        XM: device(xat(-1), y, z, core),
        YP: device(x, yat(1), z, core),
        YM: device(x, yat(-1), z, core),
        PR: device(x, y, z, other),
    }
    weights = {(G, 0): g0, (U, 0): u0, (G, 1): g1, (U, 1): u1}
    turned = {(G, 0): gt0, (U, 0): ut0, (G, 1): gt1, (U, 1): ut1}
    talls = (t0, t1)
    pairs, fars, nears = (pair0, pair1), (far0, far1), (near0, near1)
    dist = lax.rem(z + NZ - tp, NZ)

    def rows_at(ref, row, half):
        if half is None:
            return ref.at[pl.ds(pl.multiple_of(row, 64), 64), :]
        return ref.at[pl.ds(pl.multiple_of(row + 32 * half, 32), 32), :]

    def refs(c, sender):
        dz, dx, dy = STEP[c.link] if sender else (0, 0, 0)
        at = c.at
        if c.buf == E:
            if "k" in at:
                return squares.at[pl.ds(zat(at["k"]) * NX, NX)], given.at[tp]
            ref = squares.at[zat(at["z"] + dz) * NX + xat(at["x"] + dx)]
            if at["half"] is not None:
                ref = ref.at[:, pl.ds(128 * at["half"], 128)]
            return ref, ref
        if c.buf in (G, U):
            row = (zat(at["z"] + dz) * NX + xat(at["x"] + dx)) * 64
            ref = rows_at(weights[c.buf, at["layer"]], row, at["half"])
            return ref, ref
        if c.buf == D:
            n = 8 // CHUNKS
            ref = d1.at[xat(at.get("x", 0) + dx), pl.ds(at["chunk"] * n, n)]
            return ref, ref
        w = at["wave"]
        if c.buf == N:
            cc = other if at["core"] and not sender else core
            row, size = (yat(at["y"] + dy) * 2 + cc) * 64 + WAVE * w, WAVE
            if at["half"] is not None:
                row, size = row + WAVE // 2 * at["half"], WAVE // 2
            ref = normed.at[pl.ds(pl.multiple_of(row, WAVE // 2), size), :]
            return ref, ref
        l, wave = at["layer"], pl.ds(WAVE * w, WAVE)
        if at["kind"] == PAIRED:
            row = (yat(at["rel"]) * 2 + other) * 64 + WAVE * w
            return part.at[l, pl.ds(pl.multiple_of(row, WAVE), WAVE), :], pairs[l].at[at["rel"], wave, :]
        side = at["side"]
        if at["kind"] == FAR:
            half = WAVE // 2
            return sums.at[l, 2, pl.ds(WAVE * w + half * side, half), :], fars[l].at[side, pl.ds(half * w, half), :]
        return sums.at[l, 1 + 2 * side, wave, :], nears[l].at[side, wave, :]

    def describe(c, sender):
        src, dst = refs(c, sender)
        return pltpu.make_async_remote_copy(
            src_ref=src,
            dst_ref=dst,
            send_sem=send_sem.at[c.idx],
            recv_sem=recv_sem.at[c.idx],
            device_id=peers[c.link],
            device_id_type=MESH,
        )

    def own_copy(c, t):
        return pltpu.make_async_remote_copy(
            src_ref=stage,
            dst_ref=d1.at[x, t],
            send_sem=send_sem.at[c.idx],
            recv_sem=own_sem.at[1, t],
            device_id=device(x, z // 2, z, lax.rem(z, 2)),
            device_id_type=MESH,
        )

    def given_copy(c, t):
        src, _ = refs(c, True)
        to = zat(c.at["k"])
        return pltpu.make_async_remote_copy(
            src_ref=src,
            dst_ref=given.at[t],
            send_sem=send_sem.at[c.idx],
            recv_sem=own_sem.at[0, t],
            device_id=(gr, fs, to),
            device_id_type=MESH,
        )

    def passes(c):
        if "k" in c.at:
            return zat(c.at["k"]) != tp
        if c.buf != D or c.at["kind"] == ACROSS:
            return None
        if c.at["kind"] == OWN:
            return dist != 0
        return dist < 4 if c.link == ZP else jnp.logical_or(dist == 0, dist > 5)

    def if_so(here, act):
        if here is None:
            act()
        else:
            pl.when(here)(act)

    def is_own(c):
        return c.buf == D and c.at["kind"] == OWN

    def outgoing(c):
        return given_copy(c, tp) if "k" in c.at else own_copy(c, tp) if is_own(c) else describe(c, True)

    def send(c, here):
        if_so(here, outgoing(c).start)

    def sent(c):
        if_so(passes(c), outgoing(c).wait_send)

    seen = set()

    def arrived(key, only):
        c = plan.copies[key]
        if "k" in c.at:
            t = c.at["k"]
            if_so(tp != t, given_copy(c, t).wait_recv)
            return
        if c.buf == D and c.at["kind"] == ALONG:
            if_so(dist == (only if c.link == ZP else NZ - only), describe(c, False).wait_recv)
            return
        if (key, only) in seen or (only is None and (key, 4) in seen):
            return
        seen.add((key, only))
        if is_own(c):
            for t in range(8):
                if_so(jnp.logical_and(dist == 0, tp != t), own_copy(c, t).wait_recv)
            return
        here = None if only is None else hops == only
        if_so(here, describe(c, False).wait_recv)

    hops = jnp.minimum(dist, NZ - dist)
    eye = lax.broadcasted_iota(jnp.int32, (64, 64), 0) == lax.broadcasted_iota(jnp.int32, (64, 64), 1)

    def fold(gain, w):
        column = jnp.sum(jnp.where(eye, gain[...], 0.0), axis=1, keepdims=True)
        return (column * w[...]).astype(BF16)

    mine = pl.ds(pl.multiple_of((z * NX + x) * 64, 64), 64)

    def rows_of(r, cc, w):
        return pl.ds(pl.multiple_of((yat(r) * 2 + cc) * 64 + WAVE * w, WAVE), WAVE)

    def group(rs, w):
        return [rows_of(r, cc, w) for r in rs for cc in (0, 1)]

    loads = [
        pltpu.make_async_copy(src, dst, load_sem.at[i])
        for i, (src, dst) in enumerate(
            (
                (gain_a, gains.at[0]), (gate_a, gates.at[0]), (up_a, gates.at[1]), (down_a, depths.at[0]),
                (gain_b, gains.at[1]), (gate_b, gates.at[2]), (up_b, gates.at[3]), (down_b, depths.at[1]),
                (prompt_hbm, prompt),
            )
        )
    ]

    def begin():
        for load in loads:
            load.start()
        barrier = pltpu.get_barrier_semaphore()
        greet = [peers[k] for k in (ZP, ZM, XP, XM)]
        greet += [(gr, fs, lax.rem(tp + k, 8)) for k in range(1, 8)]
        for who in greet:
            pl.semaphore_signal(barrier, inc=1, device_id=who, device_id_type=MESH)
        for load in loads[:8]:
            load.wait()
        for i, ref in enumerate((g0, u0, g1, u1)):
            ref[mine, :] = fold(gains.at[i // 2], gates.at[i])
        squares[z * NX + x] = depths[0].astype(BF16)
        stage[...] = depths[1].astype(BF16)

        @pl.when(dist == 0)
        def _():
            d1[x, tp] = depths[1].astype(BF16)

        pl.semaphore_wait(barrier, len(greet))

    def norm():
        loads[8].wait()

        @pl.loop(0, 8)
        def _(i):
            at = pl.ds(pl.multiple_of(i * 64, 64), 64)
            normed[at, :] = normalized(prompt[at, :].astype(F32))

    def hide(l, w=None, rs=None):
        if l == 0:

            @pl.loop(0, 2)
            def _(i):
                at = pl.ds(pl.multiple_of(i * 256, 256), 256)
                hidden[at, :] = gated(normed[at, :], g0[...], u0[...])

            return
        spots = group(rs, w)
        out = gated(jnp.concatenate([normed[at, :] for at in spots], axis=0), g1[...], u1[...])
        for i, at in enumerate(spots):
            hidden[at, :] = out[WAVE * i : WAVE * (i + 1)]

    def turn(buf, l, piece):
        src, dst = weights[buf, l], turned[buf, l]

        @pl.loop(0, 4)
        def _(i):
            at = pl.ds(pl.multiple_of((piece * 4 + i) * 256, 256), 256)
            dst[:, at] = src[at, :].astype(F32).T.astype(BF16)

    def glue(l):
        if l == 0:
            for k in range(NX):
                given[tp, k] = squares[tp * NX + k]
        for t in range(8):
            blocks = [(given[t, k] if l == 0 else d1[k, t]).astype(F32) for k in range(NX)]
            rows = jnp.concatenate(blocks, axis=0)
            talls[l][:, 256 * t : 256 * (t + 1)] = rows.astype(BF16)

    def partial(l, w, rs):
        spots = group(rs, w)
        rows = jnp.concatenate([hidden[at, :] for at in spots], axis=0)
        out = jnp.dot(rows, talls[l][...], preferred_element_type=F32).astype(BF16)
        for i, at in enumerate(spots):
            part[l, at, :] = out[WAVE * i : WAVE * (i + 1)]

    def chip_sum(l, w, r):
        wave = slice(WAVE * w, WAVE * (w + 1))
        return part[l, rows_of(r, core, w), :].astype(F32) + pairs[l][r, wave, :].astype(F32)

    def add_up(l, w, r):
        total, half = chip_sum(l, w, r), WAVE // 2
        lower, upper = slice(WAVE * w, WAVE * w + half), slice(WAVE * w + half, WAVE * (w + 1))
        first, second = total[:half], total[half:]
        if r == 1:
            first = first + fars[l][0, half * w : half * (w + 1), :].astype(F32)
        if r == 3:
            second = second + fars[l][1, half * w : half * (w + 1), :].astype(F32)
        sums[l, r, lower, :] = first.astype(BF16)
        sums[l, r, upper, :] = second.astype(BF16)

    def last(l, w):
        wave = slice(WAVE * w, WAVE * (w + 1))
        total = chip_sum(l, w, 0) + nears[l][0, wave, :].astype(F32) + nears[l][1, wave, :].astype(F32)
        if l == 0:
            at = rows_of(0, core, w)
            rows = prompt[at, :].astype(F32) + 0.5 * total
            stream[wave, :] = rows
            normed[at, :] = normalized(rows)
        else:
            mixed[wave, :] = (stream[wave, :] + 0.5 * total).astype(BF16)

    work = {BEGIN: begin, NORM: norm, HIDE: hide, TURN: turn, GLUE: glue, PART: partial, SUM: add_up, LAST: last}
    for key, only in plan.sequence:
        if key in plan.copies:
            c = plan.copies[key]
            here = passes(c)
            if only is not None:
                here = hops == only if here is None else jnp.logical_and(here, hops == only)
            send(c, here)
            continue
        task = plan.tasks[key]
        for n in task.needs:
            if n in plan.copies and not (task.only == 4 and plan.copies[n].link == ZM and plan.copies[n].at.get("kind") == ALONG):
                arrived(n, task.only)
        if key[0] in work:
            work[key[0]](*key[1:])
    for c in plan.copies.values():
        sent(c)


def hand_out(*refs):
    sources, targets, sem = refs[:7], refs[7:14], refs[14]
    copies = [pltpu.make_async_copy(a, b, sem.at[i]) for i, (a, b) in enumerate(zip(sources, targets))]
    for copy in copies:
        copy.start()
    for copy in copies:
        copy.wait()


def shards(prompt, gain_first, gate_first, up_first, down_first, gain_second, gate_second, up_second, down_second):
    plan = build_plan()
    rows, width = prompt.shape
    units = gate_first.shape[1]
    depth, columns = down_first.shape
    count = len(plan.copies)
    sem, vmem = pltpu.SemaphoreType.DMA, pltpu.VMEM
    block = rows // 8
    tall = jax.ShapeDtypeStruct((units, width), BF16)
    shapes = (tall,) * 6 + (jax.ShapeDtypeStruct((block, width), BF16),)
    outs = pl.pallas_call(
        functools.partial(kernel, plan),
        out_shape=shapes,
        in_specs=[pl.BlockSpec(memory_space=pltpu.HBM)] * 9,
        out_specs=(pl.BlockSpec(memory_space=vmem),) * 7,
        scratch_shapes=[
            vmem((rows, width), BF16),
            vmem((rows, width), BF16),
            vmem((rows, units), BF16),
            vmem((2, rows, width), BF16),
            vmem((block, width), F32),
            *[vmem((width, units), BF16)] * 4,
            vmem((NX * NZ, depth, columns), BF16),
            vmem((8, NX, depth, columns), BF16),
            vmem((NX, 8, depth, columns), BF16),
            vmem((depth, columns), BF16),
            *[vmem((NY, block, width), BF16)] * 2,
            *[vmem((2, block // 2, width), BF16)] * 2,
            *[vmem((2, block, width), BF16)] * 2,
            vmem((2, NY, block, width), BF16),
            vmem((2, 1, gain_first.shape[0]), F32),
            vmem((4, *gate_first.shape), F32),
            vmem((2, depth, columns), F32),
            sem((9,)),
            sem((count,)),
            sem((count,)),
            sem((2, 8)),
        ],
        compiler_params=pltpu.CompilerParams(collective_id=0, has_side_effects=True, vmem_limit_bytes=LIMIT),
        name="handover",
    )(
        *[
            pltpu.with_memory_space_constraint(a, pltpu.HBM)
            for a in (
                prompt,
                gain_first.reshape(1, -1), gate_first, up_first, down_first,
                gain_second.reshape(1, -1), gate_second, up_second, down_second,
            )
        ],
    )
    outs = pl.pallas_call(
        hand_out,
        out_shape=shapes,
        in_specs=[pl.BlockSpec(memory_space=vmem)] * 7,
        out_specs=(pl.BlockSpec(memory_space=pl.ANY),) * 7,
        scratch_shapes=[sem((7,))],
        compiler_params=pltpu.CompilerParams(vmem_limit_bytes=16 * 1024 * 1024),
        name="hand_out",
    )(*outs)
    return (outs[0].T, outs[1].T, outs[2], outs[3].T, outs[4].T, outs[5], outs[6])


LIMIT = 44 * 1024 * 1024


def solution(mesh):
    rows = P(("gr", "fs"), None)
    block = P(("gr", "fs"), "tp")
    line = P(("gr", "fs"))
    return jax.shard_map(
        shards,
        mesh=mesh,
        in_specs=(rows, line, block, block, block, line, block, block, block),
        out_specs=(
            P(None, "tp"),
            P(None, "tp"),
            P("tp", None),
            P(None, "tp"),
            P(None, "tp"),
            P("tp", None),
            P(("gr", "fs", "tp"), None),
        ),
        check_vma=False,
    )
```

time: 110 us -> 102 us (0.927); the launches traced: 109 us -> 99.9 us
  Pallas kernels: 109 us -> 99.2 us
    pallas_call x1, Pallas kernels: 105 us -> 95.7 us  [shards(): pl.pallas_call(functools.partial(kernel, plan), out_shape=shapes, in_spec...]
where the time goes in v3:
time: 102 us; the launch traced here: 99.9 us
  Pallas kernels  99.2 us (97%)
    pallas_call x1, Pallas kernels, shards(): pl.pallas_call(functools.partial(kernel, plan), out_shape=shapes, in_spec...  95.7 us
    pallas_call x1, Pallas kernels, shards(): pl.pallas_call(hand_out, out_shape=shapes, in_specs=[pl.BlockSpec(memory_...  3.49 us

profile of v3, /device:TPU:1, one launch (start us, length us, event | category | flops | bytes accessed | tf_op | source)
XLA Modules:
  0.0 99.9 jit_solution(9202615922997610215)
XLA Ops:
  0.6 95.7 %handover.1 = (bf16[352,2048]{1,0:T(8,128)(2,1)S(1)}, bf16[352,2048]{1,0:T(8,128)(2,1)S(1)}, bf16[352,2048]{1,0:T(8,128)(2,1)S(1)}, bf16[352,2048]{1,0:T(8,128)(...) custom-call(bf16[512,2048]{1,0:T(8,128)(2,1)} %prompt_hbm.1, ...), custom_call_target="tpu_custom_call" | custom-call | tf_op jit(solution)/shard_map/handover/pallas_call | solution.py:688
  96.4 3.5 %hand_out.1 = (bf16[352,2048]{1,0:T(8,128)(2,1)}, bf16[352,2048]{1,0:T(8,128)(2,1)}, bf16[352,2048]{1,0:T(8,128)(2,1)}, bf16[352,2048]{1,0:T(8,128)(2,1)}, bf16[...) custom-call(bf16[352,2048]{1,0:T(8,128)(2,1)S(1)} %get-tuple-element.21.refs_0_, ...), custom_call_target="tpu_custom_call" | custom-call | tf_op jit(solution)/shard_map/hand_out/pallas_call | solution.py:728

commit v4 on v3

--- a/solution.py
+++ b/solution.py
@@ -16,7 +16,7 @@
 WAVE = 64 // WAVES
 GROUPS = ((2,), (1, 3), (0,))
 
-UNIT, SQUARE, DOWN, ROWS, PAIR, WIRE, NEAR = 1.08, 1.0, 2.15, 5.7, 0.5, 2.0, 1.0
+UNIT, SQUARE, DOWN, ROWS, PAIR, WIRE, NEAR = 1.15, 1.05, 2.1, 5.7, 0.5, 2.1, 1.0
 
 ZP, ZM, XP, XM, YP, YM, PR = LINKS = range(7)
 STEP = {ZP: (1, 0, 0), ZM: (-1, 0, 0), XP: (0, 1, 0), XM: (0, -1, 0), YP: (0, 0, 1), YM: (0, 0, -1), PR: (0, 0, 0)}
@@ -203,9 +203,10 @@
         return best[1]
 
 
-GATE = (PASS, G, 1, ALONG, 0, 2)
+GATE = (PASS, E, 0, ALONG, 0, 4)
+RELAY = [(PASS, U, 0, ALONG, 2, 0, 3)] * 2
 AHEAD = 2.0
-RANKS = [3, 0, -2, 8, 1, 10, 2, 0, 5, 10, 1, 36, 60, -24]
+RANKS = [1, 0, 3, 23, 1, 3, 18, 0, 29, 32, 10, 36, 30, -10]
 
 
 def rank_copies(p):
@@ -286,6 +287,10 @@
         c = p.copy((E, 0, GIVE, k), (YP, YM)[k % 2], 3.9, buf=E, layer=0, k=k)
         p.task((PASS, E, 0, GIVE, k), blocks[k], 0.05, [c])
         downs[0].extend([c, (PASS, E, 0, GIVE, k)])
+    for cc in (0, 1):
+        c = p.copy((E, 0, FAR, cc), YP, 3.9, buf=E, layer=0, far=cc)
+        p.task((PASS, E, 0, FAR, cc), [(PASS, E, 0, GIVE, k) for k in range(NZ)] + [RELAY[cc]], 0.05, [c])
+        downs[0].append((PASS, E, 0, FAR, cc))
     l, along = 1, {}
     for k in range(CHUNKS):
         for s, sign in signs:
@@ -367,7 +372,7 @@
     gain_b, gate_b, up_b, down_b,
     gt0, ut0, t0, gt1, ut1, t1, mixed,
     prompt, normed, hidden, part, stream,
-    g0, u0, g1, u1, squares, given, d1, stage,
+    g0, u0, g1, u1, squares, given, relayed, d1, stage,
     pair0, pair1, far0, far1, near0, near1, sums,
     gains, gates, depths,
     load_sem, send_sem, recv_sem, own_sem,
@@ -415,8 +420,6 @@
         dz, dx, dy = STEP[c.link] if sender else (0, 0, 0)
         at = c.at
         if c.buf == E:
-            if "k" in at:
-                return squares.at[pl.ds(zat(at["k"]) * NX, NX)], given.at[tp]
             ref = squares.at[zat(at["z"] + dz) * NX + xat(at["x"] + dx)]
             if at["half"] is not None:
                 ref = ref.at[:, pl.ds(128 * at["half"], 128)]
@@ -468,15 +471,27 @@
             device_id_type=MESH,
         )
 
-    def given_copy(c, t):
-        src, _ = refs(c, True)
+    onward, back = [lax.rem(y + 1 + 2 * cc, NY) for cc in (core, other)]
+
+    def given_copy(c, t, way=False):
         to = zat(c.at["k"])
         return pltpu.make_async_remote_copy(
-            src_ref=src,
+            src_ref=squares.at[pl.ds(to * NX, NX)],
+            dst_ref=relayed.at[lax.rem(to, 2)] if way else given.at[t],
+            send_sem=send_sem.at[c.idx],
+            recv_sem=own_sem.at[2, lax.rem(to, 2)] if way else own_sem.at[0, t],
+            device_id=(gr, fs, onward * 2 + core) if way else (gr, fs, to),
+            device_id_type=MESH,
+        )
+
+    def far_copy(c):
+        cc, t = c.at["far"], back * 2 + core
+        return pltpu.make_async_remote_copy(
+            src_ref=relayed.at[cc],
             dst_ref=given.at[t],
             send_sem=send_sem.at[c.idx],
             recv_sem=own_sem.at[0, t],
-            device_id=(gr, fs, to),
+            device_id=(gr, fs, onward * 2 + cc),
             device_id_type=MESH,
         )
 
@@ -499,9 +514,15 @@
         return c.buf == D and c.at["kind"] == OWN
 
     def outgoing(c):
+        if "far" in c.at:
+            return far_copy(c)
         return given_copy(c, tp) if "k" in c.at else own_copy(c, tp) if is_own(c) else describe(c, True)
 
     def send(c, here):
+        if "k" in c.at:
+            opposite = lax.rem(zat(c.at["k"]) // 2 + NY - y, NY) == 2
+            if_so(opposite, given_copy(c, tp, True).start)
+            here = jnp.logical_and(here, jnp.logical_not(opposite))
         if_so(here, outgoing(c).start)
 
     def sent(c):
@@ -660,6 +681,16 @@
         for n in task.needs:
             if n in plan.copies and not (task.only == 4 and plan.copies[n].link == ZM and plan.copies[n].at.get("kind") == ALONG):
                 arrived(n, task.only)
+        if key[:2] == (PASS, E) and key[3] == FAR:
+            cc = key[4]
+            pltpu.make_async_remote_copy(
+                src_ref=relayed.at[cc],
+                dst_ref=relayed.at[cc],
+                send_sem=send_sem.at[0],
+                recv_sem=own_sem.at[2, cc],
+                device_id=peers[PR],
+                device_id_type=MESH,
+            ).wait_recv()
         if key[0] in work:
             work[key[0]](*key[1:])
     for c in plan.copies.values():
@@ -699,6 +730,7 @@
             *[vmem((width, units), BF16)] * 4,
             vmem((NX * NZ, depth, columns), BF16),
             vmem((8, NX, depth, columns), BF16),
+            vmem((2, NX, depth, columns), BF16),
             vmem((NX, 8, depth, columns), BF16),
             vmem((depth, columns), BF16),
             *[vmem((NY, block, width), BF16)] * 2,
@@ -711,7 +743,7 @@
             sem((9,)),
             sem((count,)),
             sem((count,)),
-            sem((2, 8)),
+            sem((3, 8)),
         ],
         compiler_params=pltpu.CompilerParams(collective_id=0, has_side_effects=True, vmem_limit_bytes=LIMIT),
         name="handover",

time: 102 us -> 101 us (level); the launches traced: 99.9 us -> 101 us
  Pallas kernels: 99.2 us -> 101 us
    pallas_call x1, Pallas kernels: 95.7 us -> 97.2 us  [shards(): pl.pallas_call(functools.partial(kernel, plan), out_shape=shapes, in_spec...]
where the time goes in v4:
time: 101 us
  Pallas kernels  101 us (100%)
    pallas_call x1, Pallas kernels, shards(): pl.pallas_call(functools.partial(kernel, plan), out_shape=shapes, in_spec...  97.2 us
    pallas_call x1, Pallas kernels, shards(): pl.pallas_call(hand_out, out_shape=shapes, in_specs=[pl.BlockSpec(memory_...  3.49 us

profile of v4, /device:TPU:1, one launch (start us, length us, event | category | flops | bytes accessed | tf_op | source)
XLA Modules:
  0.0 101.3 jit_solution(315070171667393626)
XLA Ops:
  0.6 97.2 %handover.1 = (bf16[352,2048]{1,0:T(8,128)(2,1)S(1)}, bf16[352,2048]{1,0:T(8,128)(2,1)S(1)}, bf16[352,2048]{1,0:T(8,128)(2,1)S(1)}, bf16[352,2048]{1,0:T(8,128)(...) custom-call(bf16[512,2048]{1,0:T(8,128)(2,1)} %prompt_hbm.1, ...), custom_call_target="tpu_custom_call" | custom-call | tf_op jit(solution)/shard_map/handover/pallas_call | solution.py:719
  97.8 3.5 %hand_out.1 = (bf16[352,2048]{1,0:T(8,128)(2,1)}, bf16[352,2048]{1,0:T(8,128)(2,1)}, bf16[352,2048]{1,0:T(8,128)(2,1)}, bf16[352,2048]{1,0:T(8,128)(2,1)}, bf16[...) custom-call(bf16[352,2048]{1,0:T(8,128)(2,1)S(1)} %get-tuple-element.21.refs_0_, ...), custom_call_target="tpu_custom_call" | custom-call | tf_op jit(solution)/shard_map/hand_out/pallas_call | solution.py:760

commit v5 on v4

--- a/solution.py
+++ b/solution.py
@@ -112,11 +112,11 @@
             now, _, k, link, what = heapq.heappop(events)
             if link is not None:
                 queue = pending[k, link]
-                if queue and now >= free.get((k, link), 0.0) - AHEAD - 1e-9:
+                if queue and now >= free.get((k, link), 0.0) - ahead(queue[0][0]) - 1e-9:
                     _, _, key, only = heapq.heappop(queue)
                     start(k, key, only, now)
                 if queue:
-                    at_time(max(now, free[k, link] - AHEAD), k, link, None)
+                    at_time(max(now, free.get((k, link), 0.0) - ahead(queue[0][0])), k, link, None)
                 continue
             for t in users.get(what, ()) if what is not None else ():
                 if what in left[k].get(t, ()):
@@ -130,7 +130,7 @@
                     if self.starts_here(copy, k[0]):
                         self.count += 1
                         heapq.heappush(pending.setdefault((k, copy.link), []), (copy.rank, self.count, key, task.only))
-                        at_time(max(now, free.get((k, copy.link), 0.0) - AHEAD), k, copy.link, None)
+                        at_time(max(now, free.get((k, copy.link), 0.0) - ahead(copy.rank)), k, copy.link, None)
             if now < busy[k]:
                 continue
             if fixed is None:
@@ -203,10 +203,15 @@
         return best[1]
 
 
-GATE = (PASS, E, 0, ALONG, 0, 4)
-RELAY = [(PASS, U, 0, ALONG, 2, 0, 3)] * 2
-AHEAD = 2.0
-RANKS = [1, 0, 3, 23, 1, 3, 18, 0, 29, 32, 10, 36, 30, -10]
+GIVEN = 4.5
+GATE = (PASS, E, 0, ALONG, 0, 1)
+RELAY = [(E, 0, GIVE, 4)] * 2
+AHEAD = 1.0
+RANKS = [0, 0, -3, 23, 1, 3, 18, 20, 29, 34, 31, 37, 30, -50]
+
+
+def ahead(rank):
+    return AHEAD if rank >= 0 else 9.0
 
 
 def rank_copies(p):
@@ -284,11 +289,11 @@
                     p.task((PASS, U, l, ALONG, column, t, step), [(U, l, ALONG, column, t, step)], 0.03, [c])
 
     for k in range(NZ):
-        c = p.copy((E, 0, GIVE, k), (YP, YM)[k % 2], 3.9, buf=E, layer=0, k=k)
+        c = p.copy((E, 0, GIVE, k), (YP, YM)[k % 2], GIVEN, buf=E, layer=0, k=k)
         p.task((PASS, E, 0, GIVE, k), blocks[k], 0.05, [c])
         downs[0].extend([c, (PASS, E, 0, GIVE, k)])
     for cc in (0, 1):
-        c = p.copy((E, 0, FAR, cc), YP, 3.9, buf=E, layer=0, far=cc)
+        c = p.copy((E, 0, FAR, cc), (YP, YM)[cc], GIVEN, buf=E, layer=0, far=cc)
         p.task((PASS, E, 0, FAR, cc), [(PASS, E, 0, GIVE, k) for k in range(NZ)] + [RELAY[cc]], 0.05, [c])
         downs[0].append((PASS, E, 0, FAR, cc))
     l, along = 1, {}
@@ -679,6 +684,8 @@
             continue
         task = plan.tasks[key]
         for n in task.needs:
+            if key[:2] == (PASS, E) and key[3] == FAR:
+                continue
             if n in plan.copies and not (task.only == 4 and plan.copies[n].link == ZM and plan.copies[n].at.get("kind") == ALONG):
                 arrived(n, task.only)
         if key[:2] == (PASS, E) and key[3] == FAR:

time: 101 us -> 99.6 us (0.986)
  Pallas kernels: 101 us -> 98.8 us
    pallas_call x1, Pallas kernels: 97.2 us -> 95.3 us  [shards(): pl.pallas_call(functools.partial(kernel, plan), out_shape=shapes, in_spec...]
where the time goes in v5:
time: 99.6 us; the launch traced here: 99.5 us
  Pallas kernels  98.8 us (99%)
    pallas_call x1, Pallas kernels, shards(): pl.pallas_call(functools.partial(kernel, plan), out_shape=shapes, in_spec...  95.3 us
    pallas_call x1, Pallas kernels, shards(): pl.pallas_call(hand_out, out_shape=shapes, in_specs=[pl.BlockSpec(memory_...  3.49 us

profile of v5, /device:TPU:1, one launch (start us, length us, event | category | flops | bytes accessed | tf_op | source)
XLA Modules:
  0.0 99.5 jit_solution(2607616935333821813)
XLA Ops:
  0.6 95.3 %handover.1 = (bf16[352,2048]{1,0:T(8,128)(2,1)S(1)}, bf16[352,2048]{1,0:T(8,128)(2,1)S(1)}, bf16[352,2048]{1,0:T(8,128)(2,1)S(1)}, bf16[352,2048]{1,0:T(8,128)(...) custom-call(bf16[512,2048]{1,0:T(8,128)(2,1)} %prompt_hbm.1, ...), custom_call_target="tpu_custom_call" | custom-call | tf_op jit(solution)/shard_map/handover/pallas_call | solution.py:726
  96.0 3.5 %hand_out.1 = (bf16[352,2048]{1,0:T(8,128)(2,1)}, bf16[352,2048]{1,0:T(8,128)(2,1)}, bf16[352,2048]{1,0:T(8,128)(2,1)}, bf16[352,2048]{1,0:T(8,128)(2,1)}, bf16[...) custom-call(bf16[352,2048]{1,0:T(8,128)(2,1)S(1)} %get-tuple-element.21.refs_0_, ...), custom_call_target="tpu_custom_call" | custom-call | tf_op jit(solution)/shard_map/hand_out/pallas_call | solution.py:767

commit v6 on v5

--- a/solution.py
+++ b/solution.py
@@ -205,7 +205,7 @@
 
 GIVEN = 4.5
 GATE = (PASS, E, 0, ALONG, 0, 1)
-RELAY = [(E, 0, GIVE, 4)] * 2
+RELAY = [(E, 0, GIVE, 4, 2)] * 2
 AHEAD = 1.0
 RANKS = [0, 0, -3, 23, 1, 3, 18, 20, 29, 34, 31, 37, 30, -50]
 
@@ -251,7 +251,7 @@
             key = (buf, l, *tag)
             unit = SQUARE if buf == E else UNIT
             p.copy(key, link, unit * (1.0 if half is None else 0.5), buf=buf, layer=l, z=zrel, x=xrel, half=half)
-            (blocks.setdefault(zrel % NZ, []) if buf == E else whole[l]).append(key)
+            (blocks.setdefault((zrel % NZ, xrel % NX), []) if buf == E else whole[l]).append(key)
             return key
 
         z_first = (G, E) if l == 0 else (G,)
@@ -289,12 +289,13 @@
                     p.task((PASS, U, l, ALONG, column, t, step), [(U, l, ALONG, column, t, step)], 0.03, [c])
 
     for k in range(NZ):
-        c = p.copy((E, 0, GIVE, k), (YP, YM)[k % 2], GIVEN, buf=E, layer=0, k=k)
-        p.task((PASS, E, 0, GIVE, k), blocks[k], 0.05, [c])
-        downs[0].extend([c, (PASS, E, 0, GIVE, k)])
+        for j in range(NX):
+            c = p.copy((E, 0, GIVE, k, j), (YP, YM)[k % 2], GIVEN / NX, buf=E, layer=0, k=k, x=j)
+            p.task((PASS, E, 0, GIVE, k, j), blocks.get((k, j), []) + [(START, 0)], 0.04, [c])
+            downs[0].extend([c, (PASS, E, 0, GIVE, k, j)])
     for cc in (0, 1):
         c = p.copy((E, 0, FAR, cc), (YP, YM)[cc], GIVEN, buf=E, layer=0, far=cc)
-        p.task((PASS, E, 0, FAR, cc), [(PASS, E, 0, GIVE, k) for k in range(NZ)] + [RELAY[cc]], 0.05, [c])
+        p.task((PASS, E, 0, FAR, cc), [(PASS, E, 0, GIVE, k, j) for k in range(NZ) for j in range(NX)] + [RELAY[cc]], 0.05, [c])
         downs[0].append((PASS, E, 0, FAR, cc))
     l, along = 1, {}
     for k in range(CHUNKS):
@@ -476,13 +477,18 @@
             device_id_type=MESH,
         )
 
+    def passing(ref, sem):
+        return pltpu.make_async_remote_copy(
+            src_ref=ref, dst_ref=ref, send_sem=send_sem.at[0], recv_sem=sem, device_id=peers[PR], device_id_type=MESH
+        )
+
     onward, back = [lax.rem(y + 1 + 2 * cc, NY) for cc in (core, other)]
 
     def given_copy(c, t, way=False):
         to = zat(c.at["k"])
         return pltpu.make_async_remote_copy(
-            src_ref=squares.at[pl.ds(to * NX, NX)],
-            dst_ref=relayed.at[lax.rem(to, 2)] if way else given.at[t],
+            src_ref=squares.at[to * NX + xat(c.at["x"])],
+            dst_ref=relayed.at[lax.rem(to, 2), xat(c.at["x"])] if way else given.at[t, xat(c.at["x"])],
             send_sem=send_sem.at[c.idx],
             recv_sem=own_sem.at[2, lax.rem(to, 2)] if way else own_sem.at[0, t],
             device_id=(gr, fs, onward * 2 + core) if way else (gr, fs, to),
@@ -539,7 +545,9 @@
         c = plan.copies[key]
         if "k" in c.at:
             t = c.at["k"]
-            if_so(tp != t, given_copy(c, t).wait_recv)
+            if c.at["x"] == 0:
+                whole = given.at[t]
+                if_so(tp != t, passing(whole, own_sem.at[0, t]).wait_recv)
             return
         if c.buf == D and c.at["kind"] == ALONG:
             if_so(dist == (only if c.link == ZP else NZ - only), describe(c, False).wait_recv)
@@ -689,15 +697,7 @@
             if n in plan.copies and not (task.only == 4 and plan.copies[n].link == ZM and plan.copies[n].at.get("kind") == ALONG):
                 arrived(n, task.only)
         if key[:2] == (PASS, E) and key[3] == FAR:
-            cc = key[4]
-            pltpu.make_async_remote_copy(
-                src_ref=relayed.at[cc],
-                dst_ref=relayed.at[cc],
-                send_sem=send_sem.at[0],
-                recv_sem=own_sem.at[2, cc],
-                device_id=peers[PR],
-                device_id_type=MESH,
-            ).wait_recv()
+            passing(relayed.at[key[4]], own_sem.at[2, key[4]]).wait_recv()
         if key[0] in work:
             work[key[0]](*key[1:])
     for c in plan.copies.values():

time: 99.6 us -> 102 us (1.024)
  Pallas kernels: 98.8 us -> 101 us
    pallas_call x1, Pallas kernels: 95.3 us -> 97.5 us  [shards(): pl.pallas_call(functools.partial(kernel, plan), out_shape=shapes, in_spec...]
where the time goes in v6:
time: 102 us
  Pallas kernels  101 us (99%)
    pallas_call x1, Pallas kernels, shards(): pl.pallas_call(functools.partial(kernel, plan), out_shape=shapes, in_spec...  97.5 us
    pallas_call x1, Pallas kernels, shards(): pl.pallas_call(hand_out, out_shape=shapes, in_specs=[pl.BlockSpec(memory_...  3.49 us

profile of v6, /device:TPU:1, one launch (start us, length us, event | category | flops | bytes accessed | tf_op | source)
XLA Modules:
  0.0 101.6 jit_solution(654101885949384537)
XLA Ops:
  0.6 97.5 %handover.1 = (bf16[352,2048]{1,0:T(8,128)(2,1)S(1)}, bf16[352,2048]{1,0:T(8,128)(2,1)S(1)}, bf16[352,2048]{1,0:T(8,128)(2,1)S(1)}, bf16[352,2048]{1,0:T(8,128)(...) custom-call(bf16[512,2048]{1,0:T(8,128)(2,1)} %prompt_hbm.1, ...), custom_call_target="tpu_custom_call" | custom-call | tf_op jit(solution)/shard_map/handover/pallas_call | solution.py:726
  98.1 3.5 %hand_out.1 = (bf16[352,2048]{1,0:T(8,128)(2,1)}, bf16[352,2048]{1,0:T(8,128)(2,1)}, bf16[352,2048]{1,0:T(8,128)(2,1)}, bf16[352,2048]{1,0:T(8,128)(2,1)}, bf16[...) custom-call(bf16[352,2048]{1,0:T(8,128)(2,1)S(1)} %get-tuple-element.21.refs_0_, ...), custom_call_target="tpu_custom_call" | custom-call | tf_op jit(solution)/shard_map/hand_out/pallas_call | solution.py:767
